TPU v7x, 32 devices: a whole 2x2x4 slice. The times are simulated.
32 devices in a mesh: sp: 8 (over z, x), tp: 4 (over y, core).
Axes of the slice: x: 2, y: 2, z: 4, core: 2. Of those that a mesh axis runs over, the one named last changes fastest.
Arguments:
- residual: bfloat16 [8192, 2048], P('sp'), may hold values from -6 to 6
- query: bfloat16 [8192, 1024], P('sp', 'tp'), may hold values from -6 to 6
- key: bfloat16 [8192, 256], P('sp', 'tp'), may hold values from -6 to 6
- value: bfloat16 [8192, 256], P('sp', 'tp'), may hold values from -6 to 6
- sink: float32 [16], P('tp'), may hold values from 3 to 9
- norm_gain: float32 [2048], replicated, may hold values from 0.1 to 1.9
- w_out: bfloat16 [1024, 2048], P('tp'), may hold values from -1.5 to 1.5
- w_gate: bfloat16 [2048, 4096], P('sp', 'tp'), may hold values from -0.125 to 0.125
- w_value: bfloat16 [2048, 4096], P('sp', 'tp'), may hold values from -0.125 to 0.125
- conv_gate: bfloat16 [3, 4096], P(None, 'tp'), may hold values from -3 to 3
- conv_value: bfloat16 [3, 4096], P(None, 'tp'), may hold values from -3 to 3
- w_down: bfloat16 [4096, 2048], P('tp', 'sp'), may hold values from -0.09375 to 0.09375
Outputs:
- layer_out: bfloat16 [8192, 2048], P(('sp', 'tp'))
All inputs are finite; a program needn't handle non-finite values.
Results may differ from a plain program's by a relative error of at most 0.015.
Values may be sent and summed in bfloat16 or wider, within the bound.
A program may use at most 128 MiB of HBM per device.

v0:
```python
import functools

import jax
import jax.numpy as jnp
import numpy as np
from jax import lax
from jax.experimental import pallas as pl
from jax.experimental.pallas import tpu as pltpu
from jax.sharding import PartitionSpec as P

HD = 64
WINDOW = 128


THETA = 10000.0
EPS = 1e-06


def extended(block, sides, width):
    for axis, dim in sides:
        count = lax.axis_size(axis)
        forward = [(i, i + 1) for i in range(count - 1)]
        backward = [(target, source) for source, target in forward]
        low = lax.ppermute(
            lax.slice_in_dim(block, block.shape[dim] - width, None, axis=dim), axis, forward
        )
        high = lax.ppermute(lax.slice_in_dim(block, 0, width, axis=dim), axis, backward)
        block = jnp.concatenate([low, block, high], axis=dim)
    return block


def rotate(field, positions):
    count = field.shape[0]
    parts = field.astype(jnp.float32).reshape(count, -1, HD)
    inverse = 1.0 / THETA ** (jnp.arange(0, HD, 2, dtype=jnp.float32) / HD)
    angle = positions[:, None] * inverse[None, :]
    cosine = jnp.cos(angle)[:, None, :]
    sine = jnp.sin(angle)[:, None, :]
    first = parts[..., : HD // 2]
    second = parts[..., HD // 2 :]
    turned = jnp.concatenate(
        [first * cosine - second * sine, second * cosine + first * sine], axis=-1
    )
    return turned.reshape(count, -1).astype(jnp.bfloat16)


def band_attention(queries, keys, values, sinks, start, total):
    count = queries.shape[0]
    blocks = count // WINDOW
    kv_local = keys.shape[1] // HD
    group = queries.shape[1] // (kv_local * HD)
    query_blocks = queries.reshape(blocks, WINDOW, kv_local, group, HD)
    key_band = jnp.concatenate(
        [
            keys[i * WINDOW : i * WINDOW + count].reshape(blocks, WINDOW, kv_local, HD)
            for i in range(3)
        ],
        axis=1,
    )
    value_band = jnp.concatenate(
        [
            values[i * WINDOW : i * WINDOW + count].reshape(blocks, WINDOW, kv_local, HD)
            for i in range(3)
        ],
        axis=1,
    )
    scores = jnp.einsum(
        "nqkgd,njkd->nkgqj", query_blocks, key_band, preferred_element_type=jnp.float32
    ) * HD ** (-0.5)
    block_ids = jnp.arange(blocks, dtype=jnp.int32)[:, None]
    query_pos = start + block_ids * WINDOW + jnp.arange(WINDOW, dtype=jnp.int32)[None, :]
    key_pos = start - WINDOW + block_ids * WINDOW + jnp.arange(3 * WINDOW, dtype=jnp.int32)[None, :]
    valid = (
        (key_pos[:, None, :] >= 0)
        & (key_pos[:, None, :] < total)
        & (jnp.abs(query_pos[:, :, None] - key_pos[:, None, :]) <= WINDOW)
    )
    scores = jnp.where(valid[:, None, None], scores, -1e30)
    sink_col = sinks.reshape(1, kv_local, group, 1, 1)
    top = jnp.maximum(jnp.max(scores, axis=-1, keepdims=True), sink_col)
    weights = jnp.exp(scores - top)
    denom = jnp.sum(weights, axis=-1, keepdims=True) + jnp.exp(sink_col - top)
    probs = (weights / denom).astype(jnp.bfloat16)
    out = jnp.einsum("nkgqj,njkd->nqkgd", probs, value_band, preferred_element_type=jnp.float32)
    return out.reshape(count, kv_local * group * HD).astype(jnp.bfloat16)


def rmsnorm(field, gain):
    wide = field.astype(jnp.float32)
    scale = lax.rsqrt(jnp.mean(wide * wide, axis=-1, keepdims=True) + EPS)
    return (wide * scale * gain).astype(jnp.bfloat16)


def plain_shards(
    residual,
    query,
    key,
    value,
    sink,
    norm_gain,
    w_out,
    w_gate,
    w_value,
    conv_gate,
    conv_value,
    w_down,
):
    tok_rows = query.shape[0]
    offset = lax.axis_index("sp") * tok_rows
    total = tok_rows * lax.axis_size("sp")
    share = tok_rows // lax.axis_size("tp")
    tp_index = lax.axis_index("tp")
    positions = (offset + jnp.arange(tok_rows, dtype=jnp.int32)).astype(jnp.float32)
    turned_query = rotate(query, positions)
    turned_key = rotate(key, positions)
    key_width = key.shape[1]
    band = jnp.concatenate([turned_key, value], axis=1)
    edged = extended(band, (("sp", 0),), WINDOW)
    attended = band_attention(
        turned_query, edged[:, :key_width], edged[:, key_width:], sink, offset, total
    )
    partial_value = jnp.dot(attended, w_out, preferred_element_type=jnp.float32)
    mix_full = lax.psum(partial_value.astype(jnp.bfloat16), "tp").astype(jnp.float32)
    mid_full = (residual.astype(jnp.float32) + mix_full).astype(jnp.bfloat16)
    normed = rmsnorm(mid_full, norm_gain)
    mid_rows = lax.dynamic_slice_in_dim(mid_full, tp_index * share, share, 0)
    gate_full, value_full = (
        lax.all_gather(w_gate, "sp", axis=0, tiled=True),
        lax.all_gather(w_value, "sp", axis=0, tiled=True),
    )
    gate_up = jnp.dot(normed, gate_full, preferred_element_type=jnp.float32).astype(jnp.bfloat16)
    value_up = jnp.dot(normed, value_full, preferred_element_type=jnp.float32).astype(jnp.bfloat16)
    hidden_width = gate_up.shape[1]
    stacked = jnp.concatenate([gate_up, value_up], axis=1)
    edged_up = extended(stacked, (("sp", 0),), 1).astype(jnp.float32)
    taps = jnp.concatenate([conv_gate, conv_value], axis=1).astype(jnp.float32)
    convolved = edged_up[:-2] * taps[0] + edged_up[1:-1] * taps[1] + edged_up[2:] * taps[2]
    hidden = (jax.nn.silu(convolved[:, :hidden_width]) * convolved[:, hidden_width:]).astype(
        jnp.bfloat16
    )
    terms = jnp.dot(
        hidden, lax.all_gather(w_down, "sp", axis=1, tiled=True), preferred_element_type=jnp.float32
    )
    ffn_rows = lax.psum_scatter(
        terms.astype(jnp.bfloat16), "tp", scatter_dimension=0, tiled=True
    ).astype(jnp.float32)
    return (mid_rows.astype(jnp.float32) + ffn_rows).astype(jnp.bfloat16)


F32 = jnp.float32
BF16 = jnp.bfloat16
PAIR = 2
HALVES = 2
PIECES = 2 * HALVES
EDGE = 8


def layer_kernel(
    sp,
    tp,
    q_ref,
    band_ref,
    cos_ref,
    sin_ref,
    base_ref,
    sink_ref,
    res_ref,
    gain_ref,
    wo_ref,
    wg_ref,
    wv_ref,
    tg_ref,
    tv_ref,
    wd_ref,
    out_ref,
    band,
    key_value,
    value_key,
    att,
    wo,
    wg,
    wv,
    wd,
    mid,
    normed,
    upg,
    upv,
    hidden,
    terms,
    near,
    pair_sum,
    far,
    local_sem,
    up_send,
    up_recv,
    dn_send,
    dn_recv,
    wo_send,
    wo_recv,
    att_send,
    att_recv,
    kv_send,
    kv_recv,
    edge_send,
    edge_recv,
    near_send,
    near_recv,
    far_send,
    far_recv,
):
    me = lax.axis_index("sp")
    my_tp = lax.axis_index("tp")
    tok, width = mid.shape
    share = tok // tp
    line = sp // PAIR
    place = me // PAIR
    side = me % PAIR
    mate = place * PAIR + (1 - side)
    depth = wg_ref.shape[0]
    half = depth // HALVES
    cols = wd_ref.shape[1]
    hid = wg_ref.shape[1]
    has_low = me > 0
    has_high = me < sp - 1
    can_down = place > 0
    can_up = place < line - 1
    buddy = my_tp + 1 - 2 * (my_tp % 2)
    across = lax.rem(my_tp + 2, tp)
    corner = lax.rem(buddy + 2, tp)
    peers = [buddy, across, corner]

    def remote(src, dst, send, recv, **where):
        return pltpu.make_async_remote_copy(
            src_ref=src,
            dst_ref=dst,
            send_sem=send,
            recv_sem=recv,
            device_id=where,
            device_id_type=pl.DeviceIdType.MESH,
        )

    barrier = pltpu.get_barrier_semaphore()

    def greet(**where):
        pl.semaphore_signal(
            barrier, inc=1, device_id=where, device_id_type=pl.DeviceIdType.MESH
        )

    greet(sp=mate)
    for peer in peers:
        greet(tp=peer)
    far_low = has_low & (side == 0)
    far_high = has_high & (side == PAIR - 1)
    pl.when(far_low)(lambda: greet(sp=me - 1))
    pl.when(far_high)(lambda: greet(sp=me + 1))
    pl.when(can_down)(lambda: greet(sp=me - PAIR))
    pl.when(can_up)(lambda: greet(sp=me + PAIR))
    count = tp
    for able in (far_low, far_high, can_down, can_up):
        count = count + jnp.where(able, 1, 0)
    pl.semaphore_wait(barrier, count)

    def up_slot(kind, block):
        start = pl.multiple_of(block * depth + kind % HALVES * half, half)
        return (wg, wv)[kind // HALVES].at[pl.ds(start, half), :]

    def up_copy(kind, block, way, own=False):
        target = (me - PAIR, me + PAIR, mate)[way]
        slot = up_slot(kind, block)
        return remote(
            (wg_ref, wv_ref)[kind // HALVES].at[pl.ds(kind % HALVES * half, half), :]
            if own
            else slot,
            slot,
            up_send.at[kind, block, way],
            up_recv.at[kind, block],
            sp=target,
        )

    def dn_copy(block, way, own=False):
        target = (me - PAIR, me + PAIR, mate)[way]
        slot = wd.at[block]
        return remote(
            wd_ref if own else slot, slot, dn_send.at[block, way], dn_recv.at[block], sp=target
        )

    def candidate(c):
        distance = (c + 1) // 2
        there = jnp.where(c % 2 == 1, place + distance, place - distance)
        valid = (there >= 0) & (there < line)
        above = there > place
        return there, valid, above

    def distance_of(there):
        return jnp.where(there > place, there - place, place - there)

    def up_rows(ref):
        return ref.at[pl.ds(pl.multiple_of(me * depth, depth), depth), :]

    own_local = [
        pltpu.make_async_copy(wg_ref, up_rows(wg), local_sem.at[0]),
        pltpu.make_async_copy(wv_ref, up_rows(wv), local_sem.at[1]),
        pltpu.make_async_copy(wd_ref, wd.at[me], local_sem.at[2]),
        pltpu.make_async_copy(wo_ref, wo.at[my_tp], local_sem.at[3]),
        pltpu.make_async_copy(band_ref, band.at[pl.ds(WINDOW, tok), :], local_sem.at[4]),
        pltpu.make_async_copy(res_ref, mid, local_sem.at[5]),
    ]

    kv_low = remote(
        band_ref.at[pl.ds(0, WINDOW), :],
        band.at[pl.ds(WINDOW + tok, WINDOW), :],
        kv_send.at[0],
        kv_recv.at[1],
        sp=me - 1,
    )
    kv_high = remote(
        band_ref.at[pl.ds(tok - WINDOW, WINDOW), :],
        band.at[pl.ds(0, WINDOW), :],
        kv_send.at[1],
        kv_recv.at[0],
        sp=me + 1,
    )
    pl.when(has_low)(kv_low.start)
    pl.when(has_high)(kv_high.start)
    for copy in own_local:
        copy.start()
    for kind in range(PIECES):
        up_copy(kind, me, 2, True).start()
        pl.when(can_down)(up_copy(kind, me, 0, True).start)
        pl.when(can_up)(up_copy(kind, me, 1, True).start)
    dn_copy(me, 2, True).start()

    def wo_copy(k, own=True):
        slot = wo.at[my_tp if own else across]
        return remote(
            wo_ref if own else slot,
            slot,
            wo_send.at[k],
            wo_recv.at[my_tp if own else across],
            tp=(buddy, across, buddy)[k],
        )

    def att_copy(k):
        slot = att.at[across if k == 2 else my_tp]
        return remote(
            slot,
            slot,
            att_send.at[k],
            att_recv.at[across if k == 2 else my_tp],
            tp=(buddy, across, buddy)[k],
        )

    def arrived(ref, recv, source):
        slot = ref.at[source]
        return remote(slot, slot, wo_send.at[0], recv.at[source], tp=buddy)

    wo_copy(1).start()
    wo_copy(0).start()

    blank = jnp.zeros((WINDOW, band.shape[1]), BF16)

    @pl.when(jnp.logical_not(has_low))
    def _():
        band[pl.ds(0, WINDOW), :] = blank

    @pl.when(jnp.logical_not(has_high))
    def _():
        band[pl.ds(WINDOW + tok, WINDOW), :] = blank

    own_local[4].wait()
    pl.when(has_low)(kv_high.wait_recv)
    pl.when(has_high)(kv_low.wait_recv)
    heads = q_ref.shape[1] // HD
    span = 3 * WINDOW
    total = tok * sp
    lane = lax.broadcasted_iota(jnp.int32, (WINDOW, 2 * HD), 1)
    early = lane % HD < HD // 2
    low = lane < HD

    def turn(field, start):
        rows = pl.ds(start, WINDOW)
        base_cos = base_ref[0:1, :]
        base_sin = base_ref[1:2, :]
        cosine = base_cos * cos_ref[rows, :] - base_sin * sin_ref[rows, :]
        sine = base_sin * cos_ref[rows, :] + base_cos * sin_ref[rows, :]
        ahead = pltpu.roll(field, 2 * HD - HD // 2, 1)
        behind = pltpu.roll(field, HD // 2, 1)
        return field * cosine + jnp.where(early, -ahead, behind) * sine

    def turn_keys(i, carry):
        start = pl.multiple_of(i * WINDOW, WINDOW)
        field = band[pl.ds(start, WINDOW), :].astype(F32)
        field = jnp.where(low, turn(field, start), field)
        key_value[pl.ds(start, WINDOW), :] = field.astype(BF16)
        value_key[pl.ds(start, WINDOW), :] = pltpu.roll(field, HD, 1).astype(BF16)
        return carry

    lax.fori_loop(0, tok // WINDOW + 2, turn_keys, 0)

    def attend(i, carry):
        start = pl.multiple_of(i * WINDOW, WINDOW)
        straight = key_value[pl.ds(start, span), :]
        crossed = value_key[pl.ds(start, span), :]
        row = lax.broadcasted_iota(jnp.int32, (WINDOW, span), 0)
        col = lax.broadcasted_iota(jnp.int32, (WINDOW, span), 1)
        key_pos = col + (me * tok - WINDOW + start)
        valid = (col >= row) & (col <= row + 2 * WINDOW) & (key_pos >= 0) & (key_pos < total)

        def head(query, sink, keys, values):
            scores = lax.dot_general(
                query, keys, (((1,), (1,)), ((), ())), preferred_element_type=F32
            )
            scores = jnp.where(valid, scores, -1e30)
            top = jnp.maximum(jnp.max(scores, axis=-1, keepdims=True), sink)
            weights = jnp.exp(scores - top)
            denom = jnp.sum(weights, axis=-1, keepdims=True) + jnp.exp(sink - top)
            probs = (weights * (1.0 / denom)).astype(BF16)
            return jnp.dot(probs, values, preferred_element_type=F32)

        for h in range(0, heads, 2):
            lanes = pl.ds(h * HD, 2 * HD)
            field = q_ref[pl.ds(start, WINDOW), lanes].astype(F32)
            field = turn(field, pl.multiple_of(start + WINDOW, WINDOW)) * HD**-0.5
            even = head(
                jnp.where(low, field, 0.0).astype(BF16), sink_ref[h], straight, crossed
            )
            odd = head(
                jnp.where(low, 0.0, field).astype(BF16), sink_ref[h + 1], crossed, straight
            )
            att[my_tp, pl.ds(start, WINDOW), lanes] = jnp.where(low, even, odd).astype(BF16)
        return carry

    lax.fori_loop(0, tok // WINDOW, attend, 0)
    att_copy(1).start()
    att_copy(0).start()

    def pass_up(c, kind):
        there, valid, above = candidate(c)
        block = there * PAIR + side

        @pl.when(valid)
        def _():
            up_copy(kind, block, 2).wait_recv()
            if c > 2 or kind >= HALVES:
                up_copy(kind, block, 2).start()
            pl.when(above & can_down)(up_copy(kind, block, 0).start)
            pl.when(jnp.logical_not(above) & can_up)(up_copy(kind, block, 1).start)

    def start_down():
        pl.when(can_down)(dn_copy(me, 0, True).start)
        pl.when(can_up)(dn_copy(me, 1, True).start)

    def pass_down(c, carry):
        there, valid, above = candidate(c)
        block = there * PAIR + side

        @pl.when(valid)
        def _():
            dn_copy(block, 2).wait_recv()
            dn_copy(block, 2).start()
            pl.when(above & can_down)(dn_copy(block, 0).start)
            pl.when(jnp.logical_not(above) & can_up)(dn_copy(block, 1).start)

        return carry

    for kind in range(PIECES):
        for c in (1, 2):
            pass_up(c, kind)
    for kind in range(HALVES):
        up_copy(kind, mate, 2).wait_recv()
        pl.when(can_down)(up_copy(kind, mate, 0).start)
        pl.when(can_up)(up_copy(kind, mate, 1).start)
    arrived(wo, wo_recv, across).wait_recv()
    wo_copy(2, False).start()
    arrived(att, att_recv, across).wait_recv()
    att_copy(2).start()
    for kind in range(PIECES):
        for c in (3, 4):
            if c < 2 * line - 1:
                pass_up(c, kind)
    start_down()

    own_local[3].wait()
    own_local[5].wait()
    for source in (buddy, corner):
        arrived(wo, wo_recv, source).wait_recv()
        arrived(att, att_recv, source).wait_recv()
    tile = tok // 4
    piece = 512

    def mix(i, carry):
        rows = pl.ds(pl.multiple_of(i * tile, tile), tile)
        squares = jnp.zeros((tile, 1), F32)
        for c in range(0, width, piece):
            acc = jnp.zeros((tile, piece), F32)
            for k in range(tp):
                term = jnp.dot(
                    att[k, rows, :], wo[k, :, pl.ds(c, piece)], preferred_element_type=F32
                )
                acc = acc + term.astype(BF16).astype(F32)
            new = (mid[rows, pl.ds(c, piece)].astype(F32) + acc).astype(BF16)
            mid[rows, pl.ds(c, piece)] = new
            wide = new.astype(F32)
            squares = squares + jnp.sum(wide * wide, axis=-1, keepdims=True)
        scale = lax.rsqrt(squares * (1.0 / width) + EPS)
        for c in range(0, width, piece):
            wide = mid[rows, pl.ds(c, piece)].astype(F32)
            normed[rows, pl.ds(c, piece)] = (
                wide * scale * gain_ref[:, pl.ds(c, piece)]
            ).astype(BF16)
        return carry

    lax.fori_loop(0, 4, mix, 0)

    for c in range(5, 2 * line - 1):
        for kind in range(PIECES):
            pass_up(c, kind)
    lax.fori_loop(1, 3, pass_down, 0)

    for kind in range(2):
        own_local[kind].wait()

    def take_up(c, carry):
        there, valid, above = candidate(c)

        @pl.when(valid)
        def _():
            other = there * PAIR + (1 - side)
            for kind in range(PIECES):
                if kind < HALVES:
                    pl.when(c > 0)(up_copy(kind, other, 2).wait_recv)
                else:
                    up_copy(kind, other, 2).wait_recv()

        return carry

    lax.fori_loop(0, 2 * line - 1, take_up, 0)

    def project(i, carry):
        base = pl.multiple_of(i * tile, tile)
        left = normed[pl.ds(base, tile), :]
        rows = pl.ds(pl.multiple_of(base + EDGE, EDGE), tile)
        for weight, dest in ((wg, upg), (wv, upv)):
            for c in range(0, hid, piece):
                term = jnp.dot(left, weight[:, pl.ds(c, piece)], preferred_element_type=F32)
                dest[rows, pl.ds(c, piece)] = term.astype(BF16).astype(F32)
        return carry

    lax.fori_loop(0, 4, project, 0)

    def edge_low(kind):
        ref = (upg, upv)[kind]
        return remote(
            ref.at[pl.ds(EDGE, EDGE), :],
            ref.at[pl.ds(EDGE + tok, EDGE), :],
            edge_send.at[0, kind],
            edge_recv.at[1, kind],
            sp=me - 1,
        )

    def edge_high(kind):
        ref = (upg, upv)[kind]
        return remote(
            ref.at[pl.ds(tok, EDGE), :],
            ref.at[pl.ds(0, EDGE), :],
            edge_send.at[1, kind],
            edge_recv.at[0, kind],
            sp=me + 1,
        )

    none = jnp.zeros((EDGE, hid), F32)
    lax.fori_loop(3, min(5, 2 * line - 1), pass_down, 0)
    for kind in range(2):
        pl.when(has_low)(edge_low(kind).start)
        pl.when(has_high)(edge_high(kind).start)

    @pl.when(jnp.logical_not(has_low))
    def _():
        upg[pl.ds(0, EDGE), :] = none
        upv[pl.ds(0, EDGE), :] = none

    @pl.when(jnp.logical_not(has_high))
    def _():
        upg[pl.ds(EDGE + tok, EDGE), :] = none
        upv[pl.ds(EDGE + tok, EDGE), :] = none

    for kind in range(2):
        pl.when(has_low)(edge_high(kind).wait_recv)
        pl.when(has_high)(edge_low(kind).wait_recv)

    def gate(i, carry):
        base = pl.multiple_of(i * WINDOW, WINDOW)
        for c in range(0, hid, 256):
            lanes = pl.ds(c, 256)

            def convolve(ref, taps):
                field = ref[pl.ds(base, WINDOW + 2 * EDGE), lanes]
                taps = taps[:, lanes].astype(F32)
                return (
                    field[EDGE - 1 : EDGE - 1 + WINDOW] * taps[0:1]
                    + field[EDGE : EDGE + WINDOW] * taps[1:2]
                    + field[EDGE + 1 : EDGE + 1 + WINDOW] * taps[2:3]
                )

            g = convolve(upg, tg_ref)
            v = convolve(upv, tv_ref)
            hidden[pl.ds(base, WINDOW), lanes] = (g / (1.0 + jnp.exp(-g)) * v).astype(BF16)
        return carry

    lax.fori_loop(0, tok // WINDOW, gate, 0)

    def rows_of(owner):
        return pl.ds(pl.multiple_of(owner * share, share), share)

    def near_copy(block, k):
        return remote(
            terms.at[block, rows_of((buddy, corner)[k]), :],
            near.at[k, block],
            near_send.at[block, k],
            near_recv.at[block, k],
            tp=buddy,
        )

    def far_copy(block):
        return remote(
            pair_sum.at[block], far.at[block], far_send.at[block], far_recv.at[block], tp=across
        )

    def pass_pair(block):
        near_copy(block, 1).wait_recv()
        both = terms[block, rows_of(across), :].astype(F32) + near[1, block].astype(F32)
        pair_sum[block] = both.astype(BF16)
        far_copy(block).start()

    def process(block):
        def part(i, carry):
            rows = pl.ds(pl.multiple_of(i * tile, tile), tile)
            terms[block, rows, :] = jnp.dot(
                hidden[rows, :], wd[block], preferred_element_type=F32
            ).astype(BF16)
            return carry

        lax.fori_loop(0, 4, part, 0)
        near_copy(block, 1).start()
        near_copy(block, 0).start()

    own_local[2].wait()

    def down(c, carry):
        there, valid, above = candidate(c)
        block = there * PAIR + side

        @pl.when(valid)
        def _():
            @pl.when(c > 4)
            def _():
                pass_down(c, 0)

            process(block)

        before, was_valid, _ = candidate(jnp.maximum(c - 1, 0))

        @pl.when(was_valid & (c > 0))
        def _():
            other = before * PAIR + (1 - side)
            dn_copy(other, 2).wait_recv()
            process(other)
            pass_pair(before * PAIR + side)

        earlier, was_valid, _ = candidate(jnp.maximum(c - 2, 0))

        @pl.when(was_valid & (c > 1))
        def _():
            pass_pair(earlier * PAIR + (1 - side))

        return carry

    lax.fori_loop(0, 2 * line + 1, down, 0)

    my_rows = pl.ds(pl.multiple_of(my_tp * share, share), share)

    for block in range(sp):
        lanes = pl.ds(block * cols, cols)
        acc = mid[my_rows, lanes].astype(F32) + terms[block, my_rows, :].astype(F32)
        near_copy(block, 0).wait_recv()
        far_copy(block).wait_recv()
        acc = acc + near[0, block].astype(F32) + far[block].astype(F32)
        out_ref[:, lanes] = acc.astype(BF16)

    def drain(c, carry):
        there, valid, above = candidate(c)
        block = there * PAIR + side
        goes_down = can_down & (above | (c == 0))
        goes_up = can_up & (jnp.logical_not(above) | (c == 0))

        @pl.when(valid)
        def _():
            direct = (distance_of(there) > 1) | (c == 0)
            for kind in range(PIECES + 1):
                if kind < PIECES:
                    copy = functools.partial(up_copy, kind, block)
                else:
                    copy = functools.partial(dn_copy, block)
                pl.when(direct | (kind >= HALVES))(copy(2).wait_send)
                pl.when(goes_down)(copy(0).wait_send)
                pl.when(goes_up)(copy(1).wait_send)

        return carry

    for kind in range(HALVES):
        pl.when(can_down)(up_copy(kind, mate, 0).wait_send)
        pl.when(can_up)(up_copy(kind, mate, 1).wait_send)
    lax.fori_loop(0, 2 * line - 1, drain, 0)
    for k in range(tp - 1):
        wo_copy(k, k < 2).wait_send()
        att_copy(k).wait_send()
    pl.when(has_low)(kv_low.wait_send)
    pl.when(has_high)(kv_high.wait_send)
    for kind in range(2):
        pl.when(has_low)(edge_low(kind).wait_send)
        pl.when(has_high)(edge_high(kind).wait_send)

    def drain_rs(block, carry):
        near_copy(block, 0).wait_send()
        near_copy(block, 1).wait_send()
        far_copy(block).wait_send()
        return carry

    lax.fori_loop(0, sp, drain_rs, 0)


def kernel_shards(
    sp,
    tp,
    residual,
    query,
    key,
    value,
    sink,
    norm_gain,
    w_out,
    w_gate,
    w_value,
    conv_gate,
    conv_value,
    w_down,
):
    tok, width = residual.shape
    depth, hid = w_gate.shape
    cols = w_down.shape[1]
    heads = query.shape[1] // HD
    share = tok // tp
    offset = lax.axis_index("sp") * tok
    band = jnp.concatenate([key, value], axis=1)
    inverse = THETA ** (-(np.arange(2 * HD) % (HD // 2)) * 2.0 / HD)
    angle = (np.arange(tok + 2 * WINDOW) - WINDOW)[:, None] * inverse[None, :]
    first = offset.astype(F32) * jnp.asarray(inverse, F32)
    base = jnp.stack([jnp.cos(first), jnp.sin(first)])
    vmem = pl.BlockSpec(memory_space=pltpu.VMEM)
    smem = pl.BlockSpec(memory_space=pltpu.SMEM)
    anywhere = pl.BlockSpec(memory_space=pl.ANY)
    dma = pltpu.SemaphoreType.DMA
    return pl.pallas_call(
        functools.partial(layer_kernel, sp, tp),
        out_shape=jax.ShapeDtypeStruct((tok // tp, width), BF16),
        in_specs=[vmem] * 5 + [smem, anywhere, vmem] + [anywhere] * 3 + [vmem] * 2 + [anywhere],
        out_specs=vmem,
        scratch_shapes=[
            pltpu.VMEM((tok + 2 * WINDOW, 2 * HD), BF16),
            pltpu.VMEM((tok + 2 * WINDOW, 2 * HD), BF16),
            pltpu.VMEM((tok + 2 * WINDOW, 2 * HD), BF16),
            pltpu.VMEM((tp, tok, heads * HD), BF16),
            pltpu.VMEM((tp,) + w_out.shape, BF16),
            pltpu.VMEM((sp * depth, hid), BF16),
            pltpu.VMEM((sp * depth, hid), BF16),
            pltpu.VMEM((sp, hid, cols), BF16),
            pltpu.VMEM((tok, width), BF16),
            pltpu.VMEM((tok, width), BF16),
            pltpu.VMEM((tok + 2 * EDGE, hid), F32),
            pltpu.VMEM((tok + 2 * EDGE, hid), F32),
            pltpu.VMEM((tok, hid), BF16),
            pltpu.VMEM((sp, tok, cols), BF16),
            pltpu.VMEM((2, sp, share, cols), BF16),
            pltpu.VMEM((sp, share, cols), BF16),
            pltpu.VMEM((sp, share, cols), BF16),
            dma((6,)),
            dma((PIECES, sp, 3)),
            dma((PIECES, sp)),
            dma((sp, 3)),
            dma((sp,)),
            dma((tp - 1,)),
            dma((tp,)),
            dma((tp - 1,)),
            dma((tp,)),
            dma((2,)),
            dma((2,)),
            dma((2, 2)),
            dma((2, 2)),
            dma((sp, 2)),
            dma((sp, 2)),
            dma((sp,)),
            dma((sp,)),
        ],
        compiler_params=pltpu.CompilerParams(
            collective_id=0, has_side_effects=True, vmem_limit_bytes=66 * 1000 * 1000
        ),
        name="layer",
    )(
        query,
        band,
        jnp.asarray(np.cos(angle), F32),
        jnp.asarray(np.sin(angle), F32),
        base,
        sink,
        residual,
        norm_gain.reshape(1, -1),
        w_out,
        w_gate,
        w_value,
        conv_gate,
        conv_value,
        w_down,
    )


def solution(mesh):
    sp, tp = mesh.shape["sp"], mesh.shape["tp"]

    def shards(*args):
        if args[11].shape[1] % 128 or sp % PAIR or tp != 4 or args[2].shape[1] != HD:
            return plain_shards(*args)
        return kernel_shards(sp, tp, *args)

    return jax.shard_map(
        shards,
        mesh=mesh,
        in_specs=(
            P("sp", None),
            P("sp", "tp"),
            P("sp", "tp"),
            P("sp", "tp"),
            P("tp"),
            P(),
            P("tp", None),
            P("sp", "tp"),
            P("sp", "tp"),
            P(None, "tp"),
            P(None, "tp"),
            P("tp", "sp"),
        ),
        out_specs=P(("sp", "tp"), None),
        check_vma=False,
    )
```

profile of v0, /device:TPU:0, one launch (start us, length us, event | category | flops | bytes accessed | tf_op | source)
XLA Modules:
  0.0 167.8 jit_solution(12617112692398196545)
XLA Ops:
  0.0 0.7 fusion
  0.7 0.6 pad_maximum_fusion.1.base_ref
  1.3 1.1 copy.16
  2.4 1.1 copy.17
  3.5 0.9 pad_maximum_fusion.band_ref
  4.3 161.1 %layer.1 = bf16[256,2048]{1,0:T(8,128)(2,1)} custom-call(bf16[1024,256]{1,0:T(8,128)(2,1)} %q_ref.1, bf16[1024,128]{1,0:T(8,128)(2,1)} %pad_maximum_fusion.band_ref, f32[1280,128]{1,0:T(8,128)} %constant.15.clone.cos_ref, f32[1280,128]{1,0:T(8,128)} %constant.16.clone.sin_ref, f32[2,128]{1,0:T(2,128)} %pad_maximum_fusion.1.base_ref, f32[4]{0:T(128)} %sink_ref.1, ...), custom_call_target="tpu_custom_call" | custom-call | tf_op jit(solution)/shard_map/layer/pallas_call | solution.py:763
  165.5 2.3 %copy.19 = bf16[256,2048]{1,0:T(8,128)(2,1)} copy(bf16[256,2048]{1,0:T(8,128)(2,1)} %layer.1) | data formatting | bytes 2097152
where the time goes:
time: 168 us
  Pallas kernels  161 us (96%)
  local copies, waits for them, and re-layouts  4.45 us (3%)
  other arithmetic  2.15 us (1%)
    pallas_call x1, Pallas kernels, kernel_shards(): pl.pallas_call(functools.partial(layer_kernel, sp, tp), out_shape=jax.Sha...  161 us
    unnamed x3, local copies, waits for them, and re-layouts  4.45 us

commit v1 on v0

v1 whole, which is shorter than its diff:
```python
import functools

import jax
import jax.numpy as jnp
import numpy as np
from jax import lax
from jax.experimental import pallas as pl
from jax.experimental.pallas import tpu as pltpu
from jax.sharding import PartitionSpec as P

HD = 64
WINDOW = 128


THETA = 10000.0
EPS = 1e-06


def extended(block, sides, width):
    for axis, dim in sides:
        count = lax.axis_size(axis)
        forward = [(i, i + 1) for i in range(count - 1)]
        backward = [(target, source) for source, target in forward]
        low = lax.ppermute(
            lax.slice_in_dim(block, block.shape[dim] - width, None, axis=dim), axis, forward
        )
        high = lax.ppermute(lax.slice_in_dim(block, 0, width, axis=dim), axis, backward)
        block = jnp.concatenate([low, block, high], axis=dim)
    return block


def rotate(field, positions):
    count = field.shape[0]
    parts = field.astype(jnp.float32).reshape(count, -1, HD)
    inverse = 1.0 / THETA ** (jnp.arange(0, HD, 2, dtype=jnp.float32) / HD)
    angle = positions[:, None] * inverse[None, :]
    cosine = jnp.cos(angle)[:, None, :]
    sine = jnp.sin(angle)[:, None, :]
    first = parts[..., : HD // 2]
    second = parts[..., HD // 2 :]
    turned = jnp.concatenate(
        [first * cosine - second * sine, second * cosine + first * sine], axis=-1
    )
    return turned.reshape(count, -1).astype(jnp.bfloat16)


def band_attention(queries, keys, values, sinks, start, total):
    count = queries.shape[0]
    blocks = count // WINDOW
    kv_local = keys.shape[1] // HD
    group = queries.shape[1] // (kv_local * HD)
    query_blocks = queries.reshape(blocks, WINDOW, kv_local, group, HD)
    key_band = jnp.concatenate(
        [
            keys[i * WINDOW : i * WINDOW + count].reshape(blocks, WINDOW, kv_local, HD)
            for i in range(3)
        ],
        axis=1,
    )
    value_band = jnp.concatenate(
        [
            values[i * WINDOW : i * WINDOW + count].reshape(blocks, WINDOW, kv_local, HD)
            for i in range(3)
        ],
        axis=1,
    )
    scores = jnp.einsum(
        "nqkgd,njkd->nkgqj", query_blocks, key_band, preferred_element_type=jnp.float32
    ) * HD ** (-0.5)
    block_ids = jnp.arange(blocks, dtype=jnp.int32)[:, None]
    query_pos = start + block_ids * WINDOW + jnp.arange(WINDOW, dtype=jnp.int32)[None, :]
    key_pos = start - WINDOW + block_ids * WINDOW + jnp.arange(3 * WINDOW, dtype=jnp.int32)[None, :]
    valid = (
        (key_pos[:, None, :] >= 0)
        & (key_pos[:, None, :] < total)
        & (jnp.abs(query_pos[:, :, None] - key_pos[:, None, :]) <= WINDOW)
    )
    scores = jnp.where(valid[:, None, None], scores, -1e30)
    sink_col = sinks.reshape(1, kv_local, group, 1, 1)
    top = jnp.maximum(jnp.max(scores, axis=-1, keepdims=True), sink_col)
    weights = jnp.exp(scores - top)
    denom = jnp.sum(weights, axis=-1, keepdims=True) + jnp.exp(sink_col - top)
    probs = (weights / denom).astype(jnp.bfloat16)
    out = jnp.einsum("nkgqj,njkd->nqkgd", probs, value_band, preferred_element_type=jnp.float32)
    return out.reshape(count, kv_local * group * HD).astype(jnp.bfloat16)


def rmsnorm(field, gain):
    wide = field.astype(jnp.float32)
    scale = lax.rsqrt(jnp.mean(wide * wide, axis=-1, keepdims=True) + EPS)
    return (wide * scale * gain).astype(jnp.bfloat16)


def plain_shards(
    residual,
    query,
    key,
    value,
    sink,
    norm_gain,
    w_out,
    w_gate,
    w_value,
    conv_gate,
    conv_value,
    w_down,
):
    tok_rows = query.shape[0]
    offset = lax.axis_index("sp") * tok_rows
    total = tok_rows * lax.axis_size("sp")
    share = tok_rows // lax.axis_size("tp")
    tp_index = lax.axis_index("tp")
    positions = (offset + jnp.arange(tok_rows, dtype=jnp.int32)).astype(jnp.float32)
    turned_query = rotate(query, positions)
    turned_key = rotate(key, positions)
    key_width = key.shape[1]
    band = jnp.concatenate([turned_key, value], axis=1)
    edged = extended(band, (("sp", 0),), WINDOW)
    attended = band_attention(
        turned_query, edged[:, :key_width], edged[:, key_width:], sink, offset, total
    )
    partial_value = jnp.dot(attended, w_out, preferred_element_type=jnp.float32)
    mix_full = lax.psum(partial_value.astype(jnp.bfloat16), "tp").astype(jnp.float32)
    mid_full = (residual.astype(jnp.float32) + mix_full).astype(jnp.bfloat16)
    normed = rmsnorm(mid_full, norm_gain)
    mid_rows = lax.dynamic_slice_in_dim(mid_full, tp_index * share, share, 0)
    gate_full, value_full = (
        lax.all_gather(w_gate, "sp", axis=0, tiled=True),
        lax.all_gather(w_value, "sp", axis=0, tiled=True),
    )
    gate_up = jnp.dot(normed, gate_full, preferred_element_type=jnp.float32).astype(jnp.bfloat16)
    value_up = jnp.dot(normed, value_full, preferred_element_type=jnp.float32).astype(jnp.bfloat16)
    hidden_width = gate_up.shape[1]
    stacked = jnp.concatenate([gate_up, value_up], axis=1)
    edged_up = extended(stacked, (("sp", 0),), 1).astype(jnp.float32)
    taps = jnp.concatenate([conv_gate, conv_value], axis=1).astype(jnp.float32)
    convolved = edged_up[:-2] * taps[0] + edged_up[1:-1] * taps[1] + edged_up[2:] * taps[2]
    hidden = (jax.nn.silu(convolved[:, :hidden_width]) * convolved[:, hidden_width:]).astype(
        jnp.bfloat16
    )
    terms = jnp.dot(
        hidden, lax.all_gather(w_down, "sp", axis=1, tiled=True), preferred_element_type=jnp.float32
    )
    ffn_rows = lax.psum_scatter(
        terms.astype(jnp.bfloat16), "tp", scatter_dimension=0, tiled=True
    ).astype(jnp.float32)
    return (mid_rows.astype(jnp.float32) + ffn_rows).astype(jnp.bfloat16)


F32 = jnp.float32
BF16 = jnp.bfloat16
PAIR = 2
EDGE = 8


def layer_kernel(
    sp,
    tp,
    q_ref,
    band_ref,
    cos_ref,
    sin_ref,
    base_ref,
    sink_ref,
    res_ref,
    gain_ref,
    wo_ref,
    wg_ref,
    wv_ref,
    tg_ref,
    tv_ref,
    wd_ref,
    out_ref,
    band,
    key_value,
    value_key,
    att,
    att_all,
    wo,
    wg,
    wv,
    wd,
    mid,
    normed,
    upg,
    upv,
    hidden,
    terms,
    near,
    pair_sum,
    first_x,
    first_y,
    sum_x,
    sum_y,
    last_x,
    last_y,
    tapg,
    tapv,
    local_sem,
    w_send,
    w_recv,
    wo_send,
    wo_recv,
    att_send,
    att_recv,
    kv_send,
    kv_recv,
    edge_send,
    edge_recv,
    n_send,
    n_recv,
    r_send,
    r_recv,
):
    me = lax.axis_index("sp")
    my_tp = lax.axis_index("tp")
    tok = q_ref.shape[0]
    share, width = mid.shape
    group = normed.shape[0]
    line = sp // PAIR
    place = me // PAIR
    side = me % PAIR
    mate = place * PAIR + (1 - side)
    depth = wg_ref.shape[0]
    wide = wg.shape[1]
    cols = wd_ref.shape[1]
    lane_half = cols // 2
    has_low = me > 0
    has_high = me < sp - 1
    can_down = place > 0
    can_up = place < line - 1
    end_down = place == 1
    end_up = place == line - 2
    row_y = my_tp // 2
    core = my_tp % 2
    buddy = my_tp + 1 - 2 * core
    across = lax.rem(my_tp + 2, tp)
    corner = lax.rem(buddy + 2, tp)

    def remote(src, dst, send, recv, **where):
        return pltpu.make_async_remote_copy(
            src_ref=src,
            dst_ref=dst,
            send_sem=send,
            recv_sem=recv,
            device_id=where,
            device_id_type=pl.DeviceIdType.MESH,
        )

    barrier = pltpu.get_barrier_semaphore()

    def greet(**where):
        pl.semaphore_signal(
            barrier, inc=1, device_id=where, device_id_type=pl.DeviceIdType.MESH
        )

    greet(sp=mate)
    for peer in (buddy, across, corner):
        greet(tp=peer)
    far_low = has_low & (side == 0)
    far_high = has_high & (side == PAIR - 1)
    pl.when(far_low)(lambda: greet(sp=me - 1))
    pl.when(far_high)(lambda: greet(sp=me + 1))
    pl.when(can_down)(lambda: greet(sp=me - PAIR))
    pl.when(can_up)(lambda: greet(sp=me + PAIR))
    count = tp
    for able in (far_low, far_high, can_down, can_up):
        count = count + jnp.where(able, 1, 0)
    pl.semaphore_wait(barrier, count)

    def w_part(kind, half):
        start = pl.multiple_of(half * wide, wide)
        if kind == 2:
            return wd_ref.at[pl.ds(start, wide), :]
        return (wg_ref, wv_ref)[kind].at[:, pl.ds(start, wide)]

    def w_slot(kind, block):
        if kind == 2:
            return wd.at[block]
        return (wg, wv)[kind].at[pl.ds(pl.multiple_of(block * depth, depth), depth), :]

    def w_copy(kind, block, way, own=False):
        slot = w_slot(kind, block)
        src = w_part(kind, 1 - side if way == 2 else side) if own else slot
        return remote(
            src,
            slot,
            w_send.at[kind, block, way],
            w_recv.at[kind, block],
            sp=(me - PAIR, me + PAIR, mate)[way],
        )

    def step(s):
        reach = jnp.minimum(place, line - 1 - place)
        far = (s + 1) // 2
        swing = jnp.where(s % 2 == 1, place + far, place - far)
        rest = jnp.where(2 * place < line - 1, s, line - 1 - s)
        there = jnp.where(s <= 2 * reach, swing, rest)
        return there, there > place

    def forwards(above):
        return (above & can_down) | (jnp.logical_not(above) & can_up)

    def block_of(there, other):
        return there * PAIR + (1 - side if other else side)

    def relay(s, kind, other):
        there, above = step(s)
        block = block_of(there, other)

        @pl.when(forwards(above))
        def _():
            w_copy(kind, block, 2).wait_recv()
            pl.when(above & can_down)(w_copy(kind, block, 0).start)
            pl.when(jnp.logical_not(above) & can_up)(w_copy(kind, block, 1).start)

    def settle(s, kind, other):
        there, above = step(s)
        block = block_of(there, other)
        pl.when(jnp.logical_not(forwards(above)))(w_copy(kind, block, 2).wait_recv)

    kv_low = remote(
        band_ref.at[pl.ds(0, WINDOW), :],
        band.at[pl.ds(WINDOW + tok, WINDOW), :],
        kv_send.at[0],
        kv_recv.at[1],
        sp=me - 1,
    )
    kv_high = remote(
        band_ref.at[pl.ds(tok - WINDOW, WINDOW), :],
        band.at[pl.ds(0, WINDOW), :],
        kv_send.at[1],
        kv_recv.at[0],
        sp=me + 1,
    )

    def shares(index, half=None):
        if half is None:
            return pl.ds(pl.multiple_of(index * share, share), share)
        size = share // 2
        return pl.ds(pl.multiple_of(index * share + half * size, size), size)

    own_local = [
        pltpu.make_async_copy(band_ref, band.at[pl.ds(WINDOW, tok), :], local_sem.at[0]),
        pltpu.make_async_copy(wo_ref, wo.at[my_tp], local_sem.at[1]),
        pltpu.make_async_copy(res_ref.at[shares(my_tp), :], mid, local_sem.at[2]),
    ] + [
        pltpu.make_async_copy(w_part(kind, side), w_slot(kind, me), local_sem.at[3 + kind])
        for kind in range(3)
    ]

    def wo_copy(k, own=True):
        slot = wo.at[my_tp if own else across]
        return remote(
            wo_ref if own else slot,
            slot,
            wo_send.at[k],
            wo_recv.at[my_tp if own else across],
            tp=(buddy, across, buddy)[k],
        )

    def arrived(ref, recv, source):
        slot = ref.at[source]
        return remote(slot, slot, wo_send.at[0], recv.at[source], tp=buddy)

    pl.when(has_low)(kv_low.start)
    pl.when(has_high)(kv_high.start)
    for copy in own_local:
        copy.start()
    for kind in range(2):
        w_copy(kind, me, 2, True).start()
        pl.when(can_down)(w_copy(kind, me, 0, True).start)
        pl.when(can_up)(w_copy(kind, me, 1, True).start)
    w_copy(2, me, 2, True).start()
    wo_copy(1).start()
    wo_copy(0).start()

    for ref, taps in ((tg_ref, tapg), (tv_ref, tapv)):
        taps[...] = jnp.where(side == 0, ref[:, 0:wide], ref[:, wide : 2 * wide]).astype(F32)

    blank = jnp.zeros((WINDOW, band.shape[1]), BF16)

    @pl.when(jnp.logical_not(has_low))
    def _():
        band[pl.ds(0, WINDOW), :] = blank

    @pl.when(jnp.logical_not(has_high))
    def _():
        band[pl.ds(WINDOW + tok, WINDOW), :] = blank

    own_local[0].wait()
    pl.when(has_low)(kv_high.wait_recv)
    pl.when(has_high)(kv_low.wait_recv)
    heads = q_ref.shape[1] // HD
    span = 3 * WINDOW
    total = tok * sp
    lane = lax.broadcasted_iota(jnp.int32, (WINDOW, 2 * HD), 1)
    early = lane % HD < HD // 2
    low = lane < HD

    def turn(field, start):
        rows = pl.ds(start, WINDOW)
        base_cos = base_ref[0:1, :]
        base_sin = base_ref[1:2, :]
        cosine = base_cos * cos_ref[rows, :] - base_sin * sin_ref[rows, :]
        sine = base_sin * cos_ref[rows, :] + base_cos * sin_ref[rows, :]
        ahead = pltpu.roll(field, 2 * HD - HD // 2, 1)
        behind = pltpu.roll(field, HD // 2, 1)
        return field * cosine + jnp.where(early, -ahead, behind) * sine

    def turn_keys(i, carry):
        start = pl.multiple_of(i * WINDOW, WINDOW)
        field = band[pl.ds(start, WINDOW), :].astype(F32)
        field = jnp.where(low, turn(field, start), field)
        key_value[pl.ds(start, WINDOW), :] = field.astype(BF16)
        value_key[pl.ds(start, WINDOW), :] = pltpu.roll(field, HD, 1).astype(BF16)
        return carry

    lax.fori_loop(0, tok // WINDOW + 2, turn_keys, 0)

    def att_copy(k):
        peer = (corner, across, buddy)[k]
        return remote(
            att.at[shares(peer), :],
            att_all.at[my_tp],
            att_send.at[k],
            att_recv.at[my_tp],
            tp=peer,
        )

    per = share // WINDOW

    def attend(i, carry):
        k = i // per
        target = jnp.where(
            k == 0, corner, jnp.where(k == 1, across, jnp.where(k == 2, buddy, my_tp))
        )
        start = pl.multiple_of(target * share + i % per * WINDOW, WINDOW)
        straight = key_value[pl.ds(start, span), :]
        crossed = value_key[pl.ds(start, span), :]
        row = lax.broadcasted_iota(jnp.int32, (WINDOW, span), 0)
        col = lax.broadcasted_iota(jnp.int32, (WINDOW, span), 1)
        key_pos = col + (me * tok - WINDOW + start)
        valid = (col >= row) & (col <= row + 2 * WINDOW) & (key_pos >= 0) & (key_pos < total)

        def head(query, sink, keys, values):
            scores = lax.dot_general(
                query, keys, (((1,), (1,)), ((), ())), preferred_element_type=F32
            )
            scores = jnp.where(valid, scores, -1e30)
            top = jnp.maximum(jnp.max(scores, axis=-1, keepdims=True), sink)
            weights = jnp.exp(scores - top)
            denom = jnp.sum(weights, axis=-1, keepdims=True) + jnp.exp(sink - top)
            probs = (weights * (1.0 / denom)).astype(BF16)
            return jnp.dot(probs, values, preferred_element_type=F32)

        for h in range(0, heads, 2):
            lanes = pl.ds(h * HD, 2 * HD)
            field = q_ref[pl.ds(start, WINDOW), lanes].astype(F32)
            field = turn(field, pl.multiple_of(start + WINDOW, WINDOW)) * HD**-0.5
            even = head(
                jnp.where(low, field, 0.0).astype(BF16), sink_ref[h], straight, crossed
            )
            odd = head(
                jnp.where(low, 0.0, field).astype(BF16), sink_ref[h + 1], crossed, straight
            )
            att[pl.ds(start, WINDOW), lanes] = jnp.where(low, even, odd).astype(BF16)
        for n in range(tp - 1):
            pl.when(i == per * (n + 1) - 1)(att_copy(n).start)

        @pl.when(i == per * 2 - 1)
        def _():
            for kind in range(2):
                w_copy(kind, mate, 2).wait_recv()
                pl.when(can_down)(w_copy(kind, mate, 0).start)
                pl.when(can_up)(w_copy(kind, mate, 1).start)
            for kind in range(2):
                for s in (1, 2):
                    if s < line:
                        relay(s, kind, False)

        return carry

    lax.fori_loop(0, tok // WINDOW, attend, 0)
    att_all[my_tp] = att[shares(my_tp), :]
    for kind in range(2):
        for s in (1, 2):
            if s < line:
                relay(s, kind, True)
    arrived(wo, wo_recv, across).wait_recv()
    wo_copy(2, False).start()

    own_local[1].wait()
    own_local[2].wait()
    for source in (buddy, across, corner):
        if source is not across:
            arrived(wo, wo_recv, source).wait_recv()
        arrived(att_all, att_recv, source).wait_recv()
    piece = 512
    mine = side * tp + my_tp
    squares = jnp.zeros((share, 1), F32)
    for c in range(0, width, piece):
        acc = jnp.zeros((share, piece), F32)
        for k in range(tp):
            term = jnp.dot(att_all[k], wo[k, :, pl.ds(c, piece)], preferred_element_type=F32)
            acc = acc + term.astype(BF16).astype(F32)
        new = (mid[:, pl.ds(c, piece)].astype(F32) + acc).astype(BF16)
        mid[:, pl.ds(c, piece)] = new
        field = new.astype(F32)
        squares = squares + jnp.sum(field * field, axis=-1, keepdims=True)
    scale = lax.rsqrt(squares * (1.0 / width) + EPS)
    for c in range(0, width, piece):
        field = mid[:, pl.ds(c, piece)].astype(F32)
        normed[shares(mine), pl.ds(c, piece)] = (
            field * scale * gain_ref[:, pl.ds(c, piece)]
        ).astype(BF16)

    from_mate = (1 - side) * tp + my_tp
    from_across = side * tp + across
    from_corner = side * tp + corner
    diagonal = (1 - side) * tp + across
    rows_sent = [
        (mine, None, "buddy"),
        (mine, None, "mate"),
        (mine, None, "across"),
        (from_mate, None, "buddy"),
        (from_mate, 0, "across"),
        (from_across, None, "buddy"),
        (from_across, 1, "mate"),
        (diagonal, 0, "buddy"),
        (diagonal, 1, "buddy"),
    ]

    def n_copy(k):
        index, half, goal = rows_sent[k]
        slot = normed.at[shares(index, half), :]
        where = {"sp": mate} if goal == "mate" else {"tp": buddy if goal == "buddy" else across}
        return remote(slot, slot, n_send.at[k], n_recv.at[index, half or 0], **where)

    def n_wait(index, half=None):
        slot = normed.at[shares(index, half), :]
        remote(slot, slot, n_send.at[0], n_recv.at[index, half or 0], tp=buddy).wait_recv()

    for k in (1, 2, 0):
        n_copy(k).start()

    def relay_all(steps, kinds, other):
        for s in steps:
            if s < line:
                for kind in kinds:
                    relay(s, kind, other)

    relay_all(range(3, line), (0, 1), False)
    relay_all(range(3, line), (0, 1), True)

    w_copy(2, mate, 2).wait_recv()

    def start_down(down, up):
        pl.when(down)(w_copy(2, me, 0, True).start)
        pl.when(up)(w_copy(2, me, 1, True).start)
        pl.when(down)(w_copy(2, mate, 0).start)
        pl.when(up)(w_copy(2, mate, 1).start)

    start_down(can_down & jnp.logical_not(end_down), can_up & jnp.logical_not(end_up))
    n_wait(from_mate)
    n_copy(4).start()
    n_copy(3).start()
    n_wait(from_across)
    n_copy(6).start()
    n_copy(5).start()
    for s in range(1, line):
        for other in (False, True):
            for kind in range(2):
                settle(s, kind, other)
    for kind in range(2):
        own_local[3 + kind].wait()
    for half in range(2):
        n_wait(diagonal, half)
        n_copy(7 + half).start()
    n_wait(side * tp + buddy)
    n_wait(from_corner)
    n_wait((1 - side) * tp + buddy)
    for half in range(2):
        n_wait((1 - side) * tp + corner, half)

    tile = share
    tiles = group // tile

    def project(i):
        base = pl.multiple_of(i * tile, tile)
        left = normed[pl.ds(base, tile), :]
        rows = pl.ds(pl.multiple_of(base + EDGE, EDGE), tile)
        for weight, dest in ((wg, upg), (wv, upv)):
            term = jnp.dot(left, weight[...], preferred_element_type=F32)
            dest[rows, :] = term.astype(BF16).astype(F32)

    def project_step(i, carry):
        project(i)
        return carry

    def edge_low(kind):
        ref = (upg, upv)[kind]
        return remote(
            ref.at[pl.ds(EDGE, EDGE), :],
            ref.at[pl.ds(EDGE + group, EDGE), :],
            edge_send.at[0, kind],
            edge_recv.at[1, kind],
            sp=me - PAIR,
        )

    def edge_high(kind):
        ref = (upg, upv)[kind]
        return remote(
            ref.at[pl.ds(group, EDGE), :],
            ref.at[pl.ds(0, EDGE), :],
            edge_send.at[1, kind],
            edge_recv.at[0, kind],
            sp=me + PAIR,
        )

    def project_edge(i, carry):
        project(i * (tiles - 1))
        return carry

    lax.fori_loop(0, 2, project_edge, 0)
    for kind in range(2):
        pl.when(can_down)(edge_low(kind).start)
        pl.when(can_up)(edge_high(kind).start)
    start_down(can_down & end_down, can_up & end_up)
    relay_all((1, 2), (2,), False)
    relay_all((1, 2), (2,), True)
    lax.fori_loop(1, tiles - 1, project_step, 0)

    none = jnp.zeros((EDGE, wide), F32)

    @pl.when(jnp.logical_not(can_down))
    def _():
        upg[pl.ds(0, EDGE), :] = none
        upv[pl.ds(0, EDGE), :] = none

    @pl.when(jnp.logical_not(can_up))
    def _():
        upg[pl.ds(EDGE + group, EDGE), :] = none
        upv[pl.ds(EDGE + group, EDGE), :] = none

    for kind in range(2):
        pl.when(can_down)(edge_high(kind).wait_recv)
        pl.when(can_up)(edge_low(kind).wait_recv)

    def gate(i, carry):
        base = pl.multiple_of(i * WINDOW, WINDOW)
        for c in range(0, wide, 256):
            lanes = pl.ds(c, 256)

            def convolve(ref, taps):
                field = ref[pl.ds(base, WINDOW + 2 * EDGE), lanes]
                return (
                    field[EDGE - 1 : EDGE - 1 + WINDOW] * taps[0:1, lanes]
                    + field[EDGE : EDGE + WINDOW] * taps[1:2, lanes]
                    + field[EDGE + 1 : EDGE + 1 + WINDOW] * taps[2:3, lanes]
                )

            g = convolve(upg, tapg)
            v = convolve(upv, tapv)
            hidden[pl.ds(base, WINDOW), lanes] = (g / (1.0 + jnp.exp(-g)) * v).astype(BF16)
        return carry

    lax.fori_loop(0, group // WINDOW, gate, 0)
    relay_all(range(3, line), (2,), False)

    front = pl.ds(0, lane_half)
    back = pl.ds(lane_half, lane_half)

    def r_copy(k, block):
        src, dst = (
            (terms.at[block, :, :, 1 - core], near.at[block]),
            (pair_sum.at[block, 1 - side, :, :, front], first_x.at[block]),
            (pair_sum.at[block, :, 1 - row_y, :, back], first_y.at[block]),
            (sum_x.at[block], last_x.at[block]),
            (sum_y.at[block], last_y.at[block]),
        )[k]
        where = ({"tp": buddy}, {"sp": mate}, {"tp": across}, {"tp": across}, {"sp": mate})[k]
        return remote(src, dst, r_send.at[k, block], r_recv.at[k, block], **where)

    def block_at(j):
        there, _ = step(j // 2)
        return there * PAIR + jnp.where(j % 2 == 0, side, 1 - side)

    def produce(j):
        block = block_at(j)

        @pl.when(j == 0)
        def _():
            own_local[5].wait()

        @pl.when(j == 2)
        def _():
            relay_all(range(3, line), (2,), True)

        @pl.when(j > 1)
        def _():
            there, above = step(j // 2)
            pl.when(jnp.logical_not(forwards(above)))(w_copy(2, block, 2).wait_recv)

        def part(i, carry):
            rows = pl.ds(pl.multiple_of(i * 2 * share, 2 * share), 2 * share)
            term = jnp.dot(hidden[rows, :], wd[block], preferred_element_type=F32)
            terms[block, i // 2, i % 2] = term.astype(BF16).reshape(2, share, cols)
            return carry

        lax.fori_loop(0, group // (2 * share), part, 0)
        r_copy(0, block).start()

    def pass_first(j):
        block = block_at(j)
        r_copy(0, block).wait_recv()
        for x in range(PAIR):
            for y in range(tp // 2):
                both = terms[block, x, y, core].astype(F32) + near[block, x, y].astype(F32)
                pair_sum[block, x, y] = both.astype(BF16)
        r_copy(1, block).start()
        r_copy(2, block).start()

    def pass_second(j):
        block = block_at(j)
        r_copy(1, block).wait_recv()
        both = pair_sum[block, side, 1 - row_y, :, front].astype(F32)
        sum_x[block] = (both + first_x[block, 1 - row_y].astype(F32)).astype(BF16)
        r_copy(3, block).start()
        r_copy(2, block).wait_recv()
        both = pair_sum[block, 1 - side, row_y, :, back].astype(F32)
        sum_y[block] = (both + first_y[block, 1 - side].astype(F32)).astype(BF16)
        r_copy(4, block).start()

    def down(j, carry):
        pl.when(j < sp)(lambda: produce(j))
        pl.when((j > 0) & (j < sp + 1))(lambda: pass_first(j - 1))
        pl.when(j > 1)(lambda: pass_second(j - 2))
        return carry

    lax.fori_loop(0, sp + 2, down, 0)

    for block in range(sp):
        r_copy(3, block).wait_recv()
        r_copy(4, block).wait_recv()
        for half in range(2):
            part = (front, back)[half]
            first = first_x[block, row_y] if half == 0 else first_y[block, side]
            last = last_x[block] if half == 0 else last_y[block]
            lanes = pl.ds(block * cols + half * lane_half, lane_half)
            acc = mid[:, lanes].astype(F32) + pair_sum[block, side, row_y, :, part].astype(F32)
            acc = acc + first.astype(F32) + last.astype(F32)
            out_ref[:, lanes] = acc.astype(BF16)

    for kind in range(3):
        w_copy(kind, me, 2, True).wait_send()
        for block in (me, mate):
            pl.when(can_down)(w_copy(kind, block, 0).wait_send)
            pl.when(can_up)(w_copy(kind, block, 1).wait_send)

    def drain(s, carry):
        there, above = step(s)
        for kind in range(3):
            for other in (False, True):
                block = block_of(there, other)
                pl.when(above & can_down)(w_copy(kind, block, 0).wait_send)
                pl.when(jnp.logical_not(above) & can_up)(w_copy(kind, block, 1).wait_send)
        return carry

    lax.fori_loop(1, line, drain, 0)
    for k in range(tp - 1):
        wo_copy(k, k < 2).wait_send()
        att_copy(k).wait_send()
    for k in range(len(rows_sent)):
        n_copy(k).wait_send()
    pl.when(has_low)(kv_low.wait_send)
    pl.when(has_high)(kv_high.wait_send)
    for kind in range(2):
        pl.when(can_down)(edge_low(kind).wait_send)
        pl.when(can_up)(edge_high(kind).wait_send)

    def drain_sums(block, carry):
        for k in range(5):
            r_copy(k, block).wait_send()
        return carry

    lax.fori_loop(0, sp, drain_sums, 0)


def kernel_shards(
    sp,
    tp,
    residual,
    query,
    key,
    value,
    sink,
    norm_gain,
    w_out,
    w_gate,
    w_value,
    conv_gate,
    conv_value,
    w_down,
):
    tok, width = residual.shape
    depth, hid = w_gate.shape
    cols = w_down.shape[1]
    heads = query.shape[1] // HD
    share = tok // tp
    wide = hid // PAIR
    group = PAIR * tok
    offset = lax.axis_index("sp") * tok
    band = jnp.concatenate([key, value], axis=1)
    inverse = THETA ** (-(np.arange(2 * HD) % (HD // 2)) * 2.0 / HD)
    angle = (np.arange(tok + 2 * WINDOW) - WINDOW)[:, None] * inverse[None, :]
    first = offset.astype(F32) * jnp.asarray(inverse, F32)
    base = jnp.stack([jnp.cos(first), jnp.sin(first)])
    vmem = pl.BlockSpec(memory_space=pltpu.VMEM)
    smem = pl.BlockSpec(memory_space=pltpu.SMEM)
    anywhere = pl.BlockSpec(memory_space=pl.ANY)
    dma = pltpu.SemaphoreType.DMA
    return pl.pallas_call(
        functools.partial(layer_kernel, sp, tp),
        out_shape=jax.ShapeDtypeStruct((tok // tp, width), BF16),
        in_specs=[vmem] * 5 + [smem, anywhere, vmem] + [anywhere] * 3 + [vmem] * 2 + [anywhere],
        out_specs=vmem,
        scratch_shapes=[
            pltpu.VMEM((tok + 2 * WINDOW, 2 * HD), BF16),
            pltpu.VMEM((tok + 2 * WINDOW, 2 * HD), BF16),
            pltpu.VMEM((tok + 2 * WINDOW, 2 * HD), BF16),
            pltpu.VMEM((tok, heads * HD), BF16),
            pltpu.VMEM((tp, share, heads * HD), BF16),
            pltpu.VMEM((tp,) + w_out.shape, BF16),
            pltpu.VMEM((sp * depth, wide), BF16),
            pltpu.VMEM((sp * depth, wide), BF16),
            pltpu.VMEM((sp, wide, cols), BF16),
            pltpu.VMEM((share, width), BF16),
            pltpu.VMEM((group, width), BF16),
            pltpu.VMEM((group + 2 * EDGE, wide), F32),
            pltpu.VMEM((group + 2 * EDGE, wide), F32),
            pltpu.VMEM((group, wide), BF16),
            pltpu.VMEM((sp, PAIR, tp // 2, 2, share, cols), BF16),
            pltpu.VMEM((sp, PAIR, tp // 2, share, cols), BF16),
            pltpu.VMEM((sp, PAIR, tp // 2, share, cols), BF16),
            pltpu.VMEM((sp, tp // 2, share, cols // 2), BF16),
            pltpu.VMEM((sp, PAIR, share, cols // 2), BF16),
            pltpu.VMEM((sp, share, cols // 2), BF16),
            pltpu.VMEM((sp, share, cols // 2), BF16),
            pltpu.VMEM((sp, share, cols // 2), BF16),
            pltpu.VMEM((sp, share, cols // 2), BF16),
            pltpu.VMEM((3, wide), F32),
            pltpu.VMEM((3, wide), F32),
            dma((6,)),
            dma((3, sp, 3)),
            dma((3, sp)),
            dma((tp - 1,)),
            dma((tp,)),
            dma((tp - 1,)),
            dma((tp,)),
            dma((2,)),
            dma((2,)),
            dma((2, 2)),
            dma((2, 2)),
            dma((9,)),
            dma((PAIR * tp, 2)),
            dma((5, sp)),
            dma((5, sp)),
        ],
        compiler_params=pltpu.CompilerParams(
            collective_id=0, has_side_effects=True, vmem_limit_bytes=66 * 1000 * 1000
        ),
        name="layer",
    )(
        query,
        band,
        jnp.asarray(np.cos(angle), F32),
        jnp.asarray(np.sin(angle), F32),
        base,
        sink,
        residual,
        norm_gain.reshape(1, -1),
        w_out,
        w_gate,
        w_value,
        conv_gate,
        conv_value,
        w_down,
    )


def solution(mesh):
    sp, tp = mesh.shape["sp"], mesh.shape["tp"]

    def shards(*args):
        if args[11].shape[1] % 256 or sp % PAIR or tp != 4 or args[2].shape[1] != HD:
            return plain_shards(*args)
        return kernel_shards(sp, tp, *args)

    return jax.shard_map(
        shards,
        mesh=mesh,
        in_specs=(
            P("sp", None),
            P("sp", "tp"),
            P("sp", "tp"),
            P("sp", "tp"),
            P("tp"),
            P(),
            P("tp", None),
            P("sp", "tp"),
            P("sp", "tp"),
            P(None, "tp"),
            P(None, "tp"),
            P("tp", "sp"),
        ),
        out_specs=P(("sp", "tp"), None),
        check_vma=False,
    )
```

time: 168 us -> 148 us (0.88)
  Pallas kernels: 161 us -> 141 us
    pallas_call x1, Pallas kernels: 161 us -> 141 us  [kernel_shards(): pl.pallas_call(functools.partial(layer_kernel, sp, tp), out_shape=jax.Sha...]
where the time goes in v1:
time: 148 us
  Pallas kernels  141 us (95%)
  local copies, waits for them, and re-layouts  4.45 us (3%)
  other arithmetic  2.15 us (1%)
    pallas_call x1, Pallas kernels, kernel_shards(): pl.pallas_call(functools.partial(layer_kernel, sp, tp), out_shape=jax.Sha...  141 us
    unnamed x3, local copies, waits for them, and re-layouts  4.45 us

profile of v1, /device:TPU:0, one launch (start us, length us, event | category | flops | bytes accessed | tf_op | source)
XLA Modules:
  0.0 147.7 jit_solution(7663866323515756419)
XLA Ops:
  0.0 0.7 fusion
  0.7 0.6 pad_maximum_fusion.1.base_ref
  1.3 1.1 copy.16
  2.4 1.1 copy.17
  3.5 0.9 pad_maximum_fusion.band_ref
  4.3 141.1 %layer.1 = bf16[256,2048]{1,0:T(8,128)(2,1)} custom-call(bf16[1024,256]{1,0:T(8,128)(2,1)} %q_ref.1, bf16[1024,128]{1,0:T(8,128)(2,1)} %pad_maximum_fusion.band_ref, f32[1280,128]{1,0:T(8,128)} %constant.15.clone.cos_ref, f32[1280,128]{1,0:T(8,128)} %constant.16.clone.sin_ref, f32[2,128]{1,0:T(2,128)} %pad_maximum_fusion.1.base_ref, f32[4]{0:T(128)} %sink_ref.1, ...), custom_call_target="tpu_custom_call" | custom-call | tf_op jit(solution)/shard_map/layer/pallas_call | solution.py:823
  145.4 2.3 %copy.19 = bf16[256,2048]{1,0:T(8,128)(2,1)} copy(bf16[256,2048]{1,0:T(8,128)(2,1)} %layer.1) | data formatting | bytes 2097152

commit v2 on v1

--- a/solution.py
+++ b/solution.py
@@ -157,10 +157,9 @@
     sp,
     tp,
     q_ref,
-    band_ref,
-    cos_ref,
-    sin_ref,
-    base_ref,
+    k_ref,
+    v_ref,
+    table_ref,
     sink_ref,
     res_ref,
     gain_ref,
@@ -171,6 +170,8 @@
     tv_ref,
     wd_ref,
     out_ref,
+    q,
+    table,
     band,
     key_value,
     value_key,
@@ -214,7 +215,7 @@
 ):
     me = lax.axis_index("sp")
     my_tp = lax.axis_index("tp")
-    tok = q_ref.shape[0]
+    tok = q.shape[0]
     share, width = mid.shape
     group = normed.shape[0]
     line = sp // PAIR
@@ -254,6 +255,11 @@
             barrier, inc=1, device_id=where, device_id_type=pl.DeviceIdType.MESH
         )
 
+    def own_band(i):
+        lanes = pl.ds(i * WINDOW, WINDOW)
+        pair = jnp.concatenate([k_ref[:, lanes], v_ref[:, lanes]], axis=0)
+        band[pl.ds((i + 1) * WINDOW, WINDOW), :] = pair.astype(F32).T.astype(BF16)
+
     greet(sp=mate)
     for peer in (buddy, across, corner):
         greet(tp=peer)
@@ -266,6 +272,14 @@
     count = tp
     for able in (far_low, far_high, can_down, can_up):
         count = count + jnp.where(able, 1, 0)
+    early_local = [
+        pltpu.make_async_copy(q_ref, q, local_sem.at[0]),
+        pltpu.make_async_copy(table_ref, table, local_sem.at[6]),
+    ]
+    for copy in early_local:
+        copy.start()
+    own_band(0)
+    own_band(tok // WINDOW - 1)
     pl.semaphore_wait(barrier, count)
 
     def w_part(kind, half):
@@ -320,14 +334,14 @@
         pl.when(jnp.logical_not(forwards(above)))(w_copy(kind, block, 2).wait_recv)
 
     kv_low = remote(
-        band_ref.at[pl.ds(0, WINDOW), :],
+        band.at[pl.ds(WINDOW, WINDOW), :],
         band.at[pl.ds(WINDOW + tok, WINDOW), :],
         kv_send.at[0],
         kv_recv.at[1],
         sp=me - 1,
     )
     kv_high = remote(
-        band_ref.at[pl.ds(tok - WINDOW, WINDOW), :],
+        band.at[pl.ds(tok, WINDOW), :],
         band.at[pl.ds(0, WINDOW), :],
         kv_send.at[1],
         kv_recv.at[0],
@@ -341,7 +355,6 @@
         return pl.ds(pl.multiple_of(index * share + half * size, size), size)
 
     own_local = [
-        pltpu.make_async_copy(band_ref, band.at[pl.ds(WINDOW, tok), :], local_sem.at[0]),
         pltpu.make_async_copy(wo_ref, wo.at[my_tp], local_sem.at[1]),
         pltpu.make_async_copy(res_ref.at[shares(my_tp), :], mid, local_sem.at[2]),
     ] + [
@@ -388,11 +401,15 @@
     def _():
         band[pl.ds(WINDOW + tok, WINDOW), :] = blank
 
-    own_local[0].wait()
+    for i in range(1, tok // WINDOW - 1):
+        own_band(i)
+    for copy in early_local:
+        copy.wait()
     pl.when(has_low)(kv_high.wait_recv)
     pl.when(has_high)(kv_low.wait_recv)
-    heads = q_ref.shape[1] // HD
+    heads = q.shape[1] // HD
     span = 3 * WINDOW
+    steps = tok + 2 * WINDOW
     total = tok * sp
     lane = lax.broadcasted_iota(jnp.int32, (WINDOW, 2 * HD), 1)
     early = lane % HD < HD // 2
@@ -400,10 +417,12 @@
 
     def turn(field, start):
         rows = pl.ds(start, WINDOW)
-        base_cos = base_ref[0:1, :]
-        base_sin = base_ref[1:2, :]
-        cosine = base_cos * cos_ref[rows, :] - base_sin * sin_ref[rows, :]
-        sine = base_sin * cos_ref[rows, :] + base_cos * sin_ref[rows, :]
+        base_cos = table[pl.ds(2 * steps + me, 1), :]
+        base_sin = table[pl.ds(2 * steps + sp + me, 1), :]
+        near_cos = table[rows, :]
+        near_sin = table[pl.ds(pl.multiple_of(steps + start, WINDOW), WINDOW), :]
+        cosine = base_cos * near_cos - base_sin * near_sin
+        sine = base_sin * near_cos + base_cos * near_sin
         ahead = pltpu.roll(field, 2 * HD - HD // 2, 1)
         behind = pltpu.roll(field, HD // 2, 1)
         return field * cosine + jnp.where(early, -ahead, behind) * sine
@@ -456,7 +475,7 @@
 
         for h in range(0, heads, 2):
             lanes = pl.ds(h * HD, 2 * HD)
-            field = q_ref[pl.ds(start, WINDOW), lanes].astype(F32)
+            field = q[pl.ds(start, WINDOW), lanes].astype(F32)
             field = turn(field, pl.multiple_of(start + WINDOW, WINDOW)) * HD**-0.5
             even = head(
                 jnp.where(low, field, 0.0).astype(BF16), sink_ref[h], straight, crossed
@@ -490,8 +509,8 @@
     arrived(wo, wo_recv, across).wait_recv()
     wo_copy(2, False).start()
 
+    own_local[0].wait()
     own_local[1].wait()
-    own_local[2].wait()
     for source in (buddy, across, corner):
         if source is not across:
             arrived(wo, wo_recv, source).wait_recv()
@@ -554,48 +573,73 @@
     relay_all(range(3, line), (0, 1), True)
 
     w_copy(2, mate, 2).wait_recv()
-
-    def start_down(down, up):
-        pl.when(down)(w_copy(2, me, 0, True).start)
-        pl.when(up)(w_copy(2, me, 1, True).start)
-        pl.when(down)(w_copy(2, mate, 0).start)
-        pl.when(up)(w_copy(2, mate, 1).start)
-
-    start_down(can_down & jnp.logical_not(end_down), can_up & jnp.logical_not(end_up))
+    inner_down = can_down & jnp.logical_not(end_down)
+    inner_up = can_up & jnp.logical_not(end_up)
+
+    def start_down(down, up, other):
+        block = mate if other else me
+        pl.when(down)(w_copy(2, block, 0, not other).start)
+        pl.when(up)(w_copy(2, block, 1, not other).start)
+
+    start_down(can_down, can_up, False)
+    start_down(inner_down, inner_up, True)
+
+    last_there, _ = step(line - 1)
+    plane = PAIR * depth
+    tail = pl.ds(pl.multiple_of(last_there * plane, plane), plane)
+    main_start = jnp.where(last_there == 0, plane, 0)
+    main = pl.ds(pl.multiple_of(main_start, plane), (line - 1) * plane)
+    tile = share
+    tiles = group // tile
+
+    def up_main(i):
+        left = normed[shares(i), main]
+        rows = pl.ds(pl.multiple_of(i * tile + EDGE, EDGE), tile)
+        for weight, dest in ((wg, upg), (wv, upv)):
+            dest[rows, :] = jnp.dot(left, weight[main, :], preferred_element_type=F32)
+
+    def up_tail(i):
+        left = normed[shares(i), tail]
+        rows = pl.ds(pl.multiple_of(i * tile + EDGE, EDGE), tile)
+        for weight, dest in ((wg, upg), (wv, upv)):
+            term = jnp.dot(left, weight[tail, :], preferred_element_type=F32)
+            dest[rows, :] = (dest[rows, :] + term).astype(BF16).astype(F32)
+
+    def settle_up(s):
+        for other in (False, True):
+            for kind in range(2):
+                settle(s, kind, other)
+
+    for s in range(1, line - 1):
+        settle_up(s)
+    for kind in range(2):
+        own_local[2 + kind].wait()
+    up_main(mine)
+    n_wait(side * tp + buddy)
+    up_main(side * tp + buddy)
     n_wait(from_mate)
     n_copy(4).start()
     n_copy(3).start()
     n_wait(from_across)
     n_copy(6).start()
     n_copy(5).start()
-    for s in range(1, line):
-        for other in (False, True):
-            for kind in range(2):
-                settle(s, kind, other)
-    for kind in range(2):
-        own_local[3 + kind].wait()
+    up_main(from_mate)
+    up_main(from_across)
+    n_wait((1 - side) * tp + buddy)
+    up_main((1 - side) * tp + buddy)
+    n_wait(from_corner)
+    up_main(from_corner)
     for half in range(2):
         n_wait(diagonal, half)
         n_copy(7 + half).start()
-    n_wait(side * tp + buddy)
-    n_wait(from_corner)
-    n_wait((1 - side) * tp + buddy)
+    up_main(diagonal)
     for half in range(2):
         n_wait((1 - side) * tp + corner, half)
-
-    tile = share
-    tiles = group // tile
-
-    def project(i):
-        base = pl.multiple_of(i * tile, tile)
-        left = normed[pl.ds(base, tile), :]
-        rows = pl.ds(pl.multiple_of(base + EDGE, EDGE), tile)
-        for weight, dest in ((wg, upg), (wv, upv)):
-            term = jnp.dot(left, weight[...], preferred_element_type=F32)
-            dest[rows, :] = term.astype(BF16).astype(F32)
-
-    def project_step(i, carry):
-        project(i)
+    up_main((1 - side) * tp + corner)
+    settle_up(line - 1)
+
+    def up_step(i, carry):
+        up_tail(i)
         return carry
 
     def edge_low(kind):
@@ -618,18 +662,15 @@
             sp=me + PAIR,
         )
 
-    def project_edge(i, carry):
-        project(i * (tiles - 1))
-        return carry
-
-    lax.fori_loop(0, 2, project_edge, 0)
+    up_tail(0)
+    up_tail(tiles - 1)
     for kind in range(2):
         pl.when(can_down)(edge_low(kind).start)
         pl.when(can_up)(edge_high(kind).start)
-    start_down(can_down & end_down, can_up & end_up)
+    start_down(can_down & end_down, can_up & end_up, True)
     relay_all((1, 2), (2,), False)
     relay_all((1, 2), (2,), True)
-    lax.fori_loop(1, tiles - 1, project_step, 0)
+    lax.fori_loop(1, tiles - 1, up_step, 0)
 
     none = jnp.zeros((EDGE, wide), F32)
 
@@ -668,14 +709,12 @@
     lax.fori_loop(0, group // WINDOW, gate, 0)
     relay_all(range(3, line), (2,), False)
 
-    front = pl.ds(0, lane_half)
-    back = pl.ds(lane_half, lane_half)
 
     def r_copy(k, block):
         src, dst = (
             (terms.at[block, :, :, 1 - core], near.at[block]),
-            (pair_sum.at[block, 1 - side, :, :, front], first_x.at[block]),
-            (pair_sum.at[block, :, 1 - row_y, :, back], first_y.at[block]),
+            (pair_sum.at[block, 0, 1 - side], first_x.at[block]),
+            (pair_sum.at[block, 1, :, 1 - row_y], first_y.at[block]),
             (sum_x.at[block], last_x.at[block]),
             (sum_y.at[block], last_y.at[block]),
         )[k]
@@ -691,7 +730,7 @@
 
         @pl.when(j == 0)
         def _():
-            own_local[5].wait()
+            own_local[4].wait()
 
         @pl.when(j == 2)
         def _():
@@ -717,38 +756,40 @@
         for x in range(PAIR):
             for y in range(tp // 2):
                 both = terms[block, x, y, core].astype(F32) + near[block, x, y].astype(F32)
-                pair_sum[block, x, y] = both.astype(BF16)
+                pair_sum[block, 0, x, y] = both[:, :lane_half].astype(BF16)
+                pair_sum[block, 1, x, y] = both[:, lane_half:].astype(BF16)
         r_copy(1, block).start()
         r_copy(2, block).start()
 
     def pass_second(j):
         block = block_at(j)
         r_copy(1, block).wait_recv()
-        both = pair_sum[block, side, 1 - row_y, :, front].astype(F32)
+        both = pair_sum[block, 0, side, 1 - row_y].astype(F32)
         sum_x[block] = (both + first_x[block, 1 - row_y].astype(F32)).astype(BF16)
         r_copy(3, block).start()
         r_copy(2, block).wait_recv()
-        both = pair_sum[block, 1 - side, row_y, :, back].astype(F32)
+        both = pair_sum[block, 1, 1 - side, row_y].astype(F32)
         sum_y[block] = (both + first_y[block, 1 - side].astype(F32)).astype(BF16)
         r_copy(4, block).start()
 
+    lag = 3
+
     def down(j, carry):
+        pl.when(j >= lag)(lambda: pass_second(j - lag))
+        pl.when((j > 0) & (j < sp + 1))(lambda: pass_first(j - 1))
         pl.when(j < sp)(lambda: produce(j))
-        pl.when((j > 0) & (j < sp + 1))(lambda: pass_first(j - 1))
-        pl.when(j > 1)(lambda: pass_second(j - 2))
         return carry
 
-    lax.fori_loop(0, sp + 2, down, 0)
+    lax.fori_loop(0, sp + lag, down, 0)
 
     for block in range(sp):
         r_copy(3, block).wait_recv()
         r_copy(4, block).wait_recv()
         for half in range(2):
-            part = (front, back)[half]
             first = first_x[block, row_y] if half == 0 else first_y[block, side]
             last = last_x[block] if half == 0 else last_y[block]
             lanes = pl.ds(block * cols + half * lane_half, lane_half)
-            acc = mid[:, lanes].astype(F32) + pair_sum[block, side, row_y, :, part].astype(F32)
+            acc = mid[:, lanes].astype(F32) + pair_sum[block, half, side, row_y].astype(F32)
             acc = acc + first.astype(F32) + last.astype(F32)
             out_ref[:, lanes] = acc.astype(BF16)
 
@@ -810,22 +851,25 @@
     share = tok // tp
     wide = hid // PAIR
     group = PAIR * tok
-    offset = lax.axis_index("sp") * tok
-    band = jnp.concatenate([key, value], axis=1)
     inverse = THETA ** (-(np.arange(2 * HD) % (HD // 2)) * 2.0 / HD)
-    angle = (np.arange(tok + 2 * WINDOW) - WINDOW)[:, None] * inverse[None, :]
-    first = offset.astype(F32) * jnp.asarray(inverse, F32)
-    base = jnp.stack([jnp.cos(first), jnp.sin(first)])
+    local = (np.arange(tok + 2 * WINDOW) - WINDOW)[:, None] * inverse[None, :]
+    first = (np.arange(sp) * tok)[:, None] * inverse[None, :]
+    table = np.concatenate([np.cos(local), np.sin(local), np.cos(first), np.sin(first)])
     vmem = pl.BlockSpec(memory_space=pltpu.VMEM)
     smem = pl.BlockSpec(memory_space=pltpu.SMEM)
     anywhere = pl.BlockSpec(memory_space=pl.ANY)
     dma = pltpu.SemaphoreType.DMA
     return pl.pallas_call(
         functools.partial(layer_kernel, sp, tp),
-        out_shape=jax.ShapeDtypeStruct((tok // tp, width), BF16),
-        in_specs=[vmem] * 5 + [smem, anywhere, vmem] + [anywhere] * 3 + [vmem] * 2 + [anywhere],
+        out_shape=pltpu.VMEM((tok // tp, width), BF16),
+        in_specs=[anywhere, vmem, vmem, anywhere, smem, anywhere, vmem]
+        + [anywhere] * 3
+        + [vmem] * 2
+        + [anywhere],
         out_specs=vmem,
         scratch_shapes=[
+            pltpu.VMEM(query.shape, BF16),
+            pltpu.VMEM(table.shape, F32),
             pltpu.VMEM((tok + 2 * WINDOW, 2 * HD), BF16),
             pltpu.VMEM((tok + 2 * WINDOW, 2 * HD), BF16),
             pltpu.VMEM((tok + 2 * WINDOW, 2 * HD), BF16),
@@ -842,7 +886,7 @@
             pltpu.VMEM((group, wide), BF16),
             pltpu.VMEM((sp, PAIR, tp // 2, 2, share, cols), BF16),
             pltpu.VMEM((sp, PAIR, tp // 2, share, cols), BF16),
-            pltpu.VMEM((sp, PAIR, tp // 2, share, cols), BF16),
+            pltpu.VMEM((sp, 2, PAIR, tp // 2, share, cols // 2), BF16),
             pltpu.VMEM((sp, tp // 2, share, cols // 2), BF16),
             pltpu.VMEM((sp, PAIR, share, cols // 2), BF16),
             pltpu.VMEM((sp, share, cols // 2), BF16),
@@ -851,7 +895,7 @@
             pltpu.VMEM((sp, share, cols // 2), BF16),
             pltpu.VMEM((3, wide), F32),
             pltpu.VMEM((3, wide), F32),
-            dma((6,)),
+            dma((7,)),
             dma((3, sp, 3)),
             dma((3, sp)),
             dma((tp - 1,)),
@@ -868,15 +912,14 @@
             dma((5, sp)),
         ],
         compiler_params=pltpu.CompilerParams(
-            collective_id=0, has_side_effects=True, vmem_limit_bytes=66 * 1000 * 1000
+            collective_id=0, has_side_effects=True, vmem_limit_bytes=62 * 1000 * 1000
         ),
         name="layer",
     )(
         query,
-        band,
-        jnp.asarray(np.cos(angle), F32),
-        jnp.asarray(np.sin(angle), F32),
-        base,
+        key.T,
+        value.T,
+        jnp.asarray(table, F32),
         sink,
         residual,
         norm_gain.reshape(1, -1),

time: 148 us -> 132 us (0.89)
  Pallas kernels: 141 us -> 131 us
  local copies, waits for them, and re-layouts: 4.45 us -> 0.97 us
  other arithmetic: 2.15 us -> 0 us
    pallas_call x1, Pallas kernels: 141 us -> 131 us  [kernel_shards(): pl.pallas_call(functools.partial(layer_kernel, sp, tp), out_shape=pltpu.V...]
    unnamed x3 -> x1, local copies, waits for them, and re-layouts: 4.45 us -> 0.97 us
where the time goes in v2:
time: 132 us
  Pallas kernels  131 us (99%)
    pallas_call x1, Pallas kernels, kernel_shards(): pl.pallas_call(functools.partial(layer_kernel, sp, tp), out_shape=pltpu.V...  131 us

profile of v2, /device:TPU:0, one launch (start us, length us, event | category | flops | bytes accessed | tf_op | source)
XLA Modules:
  0.0 132.1 jit_solution(12149739562282823100)
XLA Ops:
  0.0 131.1 %layer.1 = bf16[256,2048]{1,0:T(8,128)(2,1)S(1)} custom-call(bf16[1024,256]{1,0:T(8,128)(2,1)} %q_ref.1, bf16[64,1024]{1,0:T(8,128)(2,1)} %bitcast.3, bf16[64,1024]{1,0:T(8,128)(2,1)} %bitcast.4, f32[2576,128]{1,0:T(8,128)} %constant.2.clone.table_ref, f32[4]{0:T(128)} %sink_ref.1, bf16[1024,2048]{1,0:T(8,128)(2,1)} %res_ref.1, f32[1,2048]{1,0:T(1,128)} %bitcast.5, ...), custom_call_target="tpu_custom_call" | custom-call | tf_op jit(solution)/shard_map/layer/pallas_call | solution.py:862
  131.1 1.0 copy.15

commit v3 on v2

--- a/solution.py
+++ b/solution.py
@@ -225,7 +225,9 @@
     depth = wg_ref.shape[0]
     wide = wg.shape[1]
     cols = wd_ref.shape[1]
-    lane_half = cols // 2
+    unit = cols // PAIR
+    row_half = share // 2
+    downs = tuple(range(2, 2 + PAIR))
     has_low = me > 0
     has_high = me < sp - 1
     can_down = place > 0
@@ -274,7 +276,7 @@
         count = count + jnp.where(able, 1, 0)
     early_local = [
         pltpu.make_async_copy(q_ref, q, local_sem.at[0]),
-        pltpu.make_async_copy(table_ref, table, local_sem.at[6]),
+        pltpu.make_async_copy(table_ref, table, local_sem.at[3 + PAIR + 2]),
     ]
     for copy in early_local:
         copy.start()
@@ -284,13 +286,13 @@
 
     def w_part(kind, half):
         start = pl.multiple_of(half * wide, wide)
-        if kind == 2:
-            return wd_ref.at[pl.ds(start, wide), :]
+        if kind > 1:
+            return wd_ref.at[pl.ds(start, wide), pl.ds((kind - 2) * unit, unit)]
         return (wg_ref, wv_ref)[kind].at[:, pl.ds(start, wide)]
 
     def w_slot(kind, block):
-        if kind == 2:
-            return wd.at[block]
+        if kind > 1:
+            return wd.at[block, :, pl.ds((kind - 2) * unit, unit)]
         return (wg, wv)[kind].at[pl.ds(pl.multiple_of(block * depth, depth), depth), :]
 
     def w_copy(kind, block, way, own=False):
@@ -315,12 +317,14 @@
     def forwards(above):
         return (above & can_down) | (jnp.logical_not(above) & can_up)
 
-    def block_of(there, other):
+    def block_of(there, other, kind=0):
+        if kind > 1:
+            return there * PAIR + (1 if other else 0)
         return there * PAIR + (1 - side if other else side)
 
     def relay(s, kind, other):
         there, above = step(s)
-        block = block_of(there, other)
+        block = block_of(there, other, kind)
 
         @pl.when(forwards(above))
         def _():
@@ -330,7 +334,7 @@
 
     def settle(s, kind, other):
         there, above = step(s)
-        block = block_of(there, other)
+        block = block_of(there, other, kind)
         pl.when(jnp.logical_not(forwards(above)))(w_copy(kind, block, 2).wait_recv)
 
     kv_low = remote(
@@ -359,7 +363,7 @@
         pltpu.make_async_copy(res_ref.at[shares(my_tp), :], mid, local_sem.at[2]),
     ] + [
         pltpu.make_async_copy(w_part(kind, side), w_slot(kind, me), local_sem.at[3 + kind])
-        for kind in range(3)
+        for kind in range(2 + PAIR)
     ]
 
     def wo_copy(k, own=True):
@@ -384,7 +388,8 @@
         w_copy(kind, me, 2, True).start()
         pl.when(can_down)(w_copy(kind, me, 0, True).start)
         pl.when(can_up)(w_copy(kind, me, 1, True).start)
-    w_copy(2, me, 2, True).start()
+    for kind in downs:
+        w_copy(kind, me, 2, True).start()
     wo_copy(1).start()
     wo_copy(0).start()
 
@@ -572,17 +577,21 @@
     relay_all(range(3, line), (0, 1), False)
     relay_all(range(3, line), (0, 1), True)
 
-    w_copy(2, mate, 2).wait_recv()
+    for kind in downs:
+        w_copy(kind, mate, 2).wait_recv()
     inner_down = can_down & jnp.logical_not(end_down)
     inner_up = can_up & jnp.logical_not(end_up)
 
-    def start_down(down, up, other):
-        block = mate if other else me
-        pl.when(down)(w_copy(2, block, 0, not other).start)
-        pl.when(up)(w_copy(2, block, 1, not other).start)
-
-    start_down(can_down, can_up, False)
-    start_down(inner_down, inner_up, True)
+    def start_down(down, up, x):
+        for kind in downs:
+            for own in (True, False):
+                here = (side == x) if own else (side != x)
+                block = me if own else mate
+                pl.when(down & here)(w_copy(kind, block, 0, own).start)
+                pl.when(up & here)(w_copy(kind, block, 1, own).start)
+
+    start_down(can_down, can_up, 0)
+    start_down(inner_down, inner_up, 1)
 
     last_there, _ = step(line - 1)
     plane = PAIR * depth
@@ -667,29 +676,12 @@
     for kind in range(2):
         pl.when(can_down)(edge_low(kind).start)
         pl.when(can_up)(edge_high(kind).start)
-    start_down(can_down & end_down, can_up & end_up, True)
-    relay_all((1, 2), (2,), False)
-    relay_all((1, 2), (2,), True)
-    lax.fori_loop(1, tiles - 1, up_step, 0)
-
-    none = jnp.zeros((EDGE, wide), F32)
-
-    @pl.when(jnp.logical_not(can_down))
-    def _():
-        upg[pl.ds(0, EDGE), :] = none
-        upv[pl.ds(0, EDGE), :] = none
-
-    @pl.when(jnp.logical_not(can_up))
-    def _():
-        upg[pl.ds(EDGE + group, EDGE), :] = none
-        upv[pl.ds(EDGE + group, EDGE), :] = none
-
-    for kind in range(2):
-        pl.when(can_down)(edge_high(kind).wait_recv)
-        pl.when(can_up)(edge_low(kind).wait_recv)
-
-    def gate(i, carry):
-        base = pl.multiple_of(i * WINDOW, WINDOW)
+    start_down(can_down & end_down, can_up & end_up, 1)
+    for s in (1, 2):
+        for other in (False, True):
+            relay_all((s,), downs, other)
+
+    def gate(base):
         for c in range(0, wide, 256):
             lanes = pl.ds(c, 256)
 
@@ -704,96 +696,145 @@
             g = convolve(upg, tapg)
             v = convolve(upv, tapv)
             hidden[pl.ds(base, WINDOW), lanes] = (g / (1.0 + jnp.exp(-g)) * v).astype(BF16)
+
+    def gate_tile(i):
+        for r in range(0, tile, WINDOW):
+            gate(pl.multiple_of(i * tile + r, WINDOW))
+
+    def gate_step(i, carry):
+        gate_tile(i)
         return carry
 
-    lax.fori_loop(0, group // WINDOW, gate, 0)
-    relay_all(range(3, line), (2,), False)
-
-
-    def r_copy(k, block):
+    def up_and_gate(i, carry):
+        gate_tile(i - 2)
+        up_tail(i)
+        return carry
+
+    up_tail(1)
+    up_tail(2)
+    lax.fori_loop(3, tiles - 1, up_and_gate, 0)
+    lax.fori_loop(tiles - 3, tiles - 1, gate_step, 0)
+
+    none = jnp.zeros((EDGE, wide), F32)
+
+    @pl.when(jnp.logical_not(can_down))
+    def _():
+        upg[pl.ds(0, EDGE), :] = none
+        upv[pl.ds(0, EDGE), :] = none
+
+    @pl.when(jnp.logical_not(can_up))
+    def _():
+        upg[pl.ds(EDGE + group, EDGE), :] = none
+        upv[pl.ds(EDGE + group, EDGE), :] = none
+
+    for kind in range(2):
+        pl.when(can_down)(edge_high(kind).wait_recv)
+        pl.when(can_up)(edge_low(kind).wait_recv)
+
+    gate_tile(0)
+    gate_tile(tiles - 1)
+    relay_all(range(3, line), downs, False)
+
+    units = PAIR * sp
+
+    def r_copy(k, u):
         src, dst = (
-            (terms.at[block, :, :, 1 - core], near.at[block]),
-            (pair_sum.at[block, 0, 1 - side], first_x.at[block]),
-            (pair_sum.at[block, 1, :, 1 - row_y], first_y.at[block]),
-            (sum_x.at[block], last_x.at[block]),
-            (sum_y.at[block], last_y.at[block]),
+            (terms.at[u, :, :, 1 - core], near.at[u]),
+            (pair_sum.at[u, 0, 1 - side], first_x.at[u]),
+            (pair_sum.at[u, 1, :, 1 - row_y], first_y.at[u]),
+            (sum_x.at[u], last_x.at[u]),
+            (sum_y.at[u], last_y.at[u]),
         )[k]
         where = ({"tp": buddy}, {"sp": mate}, {"tp": across}, {"tp": across}, {"sp": mate})[k]
-        return remote(src, dst, r_send.at[k, block], r_recv.at[k, block], **where)
-
-    def block_at(j):
-        there, _ = step(j // 2)
-        return there * PAIR + jnp.where(j % 2 == 0, side, 1 - side)
+        return remote(src, dst, r_send.at[k, u], r_recv.at[k, u], **where)
+
+    def unit_at(j):
+        there, _ = step(j // (2 * PAIR))
+        return there * PAIR + j // PAIR % 2, j % PAIR
 
     def produce(j):
-        block = block_at(j)
+        block, piece = unit_at(j)
+        u = block * PAIR + piece
 
         @pl.when(j == 0)
         def _():
-            own_local[4].wait()
-
-        @pl.when(j == 2)
+            for kind in downs:
+                own_local[2 + kind].wait()
+
+        @pl.when(j == 2 * PAIR)
         def _():
-            relay_all(range(3, line), (2,), True)
-
-        @pl.when(j > 1)
+            relay_all(range(3, line), downs, True)
+
+        @pl.when((j >= 2 * PAIR) & (piece == 0))
         def _():
-            there, above = step(j // 2)
-            pl.when(jnp.logical_not(forwards(above)))(w_copy(2, block, 2).wait_recv)
-
-        def part(i, carry):
-            rows = pl.ds(pl.multiple_of(i * 2 * share, 2 * share), 2 * share)
-            term = jnp.dot(hidden[rows, :], wd[block], preferred_element_type=F32)
-            terms[block, i // 2, i % 2] = term.astype(BF16).reshape(2, share, cols)
-            return carry
-
-        lax.fori_loop(0, group // (2 * share), part, 0)
-        r_copy(0, block).start()
+            _, above = step(j // (2 * PAIR))
+
+            @pl.when(jnp.logical_not(forwards(above)))
+            def _():
+                for kind in downs:
+                    w_copy(kind, block, 2).wait_recv()
+
+        @pl.when(piece == 0)
+        def _():
+            for i in range(group // (2 * share)):
+                rows = pl.ds(i * 2 * share, 2 * share)
+                term = jnp.dot(hidden[rows, :], wd[block], preferred_element_type=F32)
+                term = term.astype(BF16)
+                for n in range(PAIR):
+                    part = term[:, n * unit : (n + 1) * unit].reshape(2, share, unit)
+                    terms[block * PAIR + n, i // 2, i % 2] = part
+
+        r_copy(0, u).start()
+
+    def unit_of(j):
+        block, piece = unit_at(j)
+        return block * PAIR + piece
 
     def pass_first(j):
-        block = block_at(j)
-        r_copy(0, block).wait_recv()
+        u = unit_of(j)
+        r_copy(0, u).wait_recv()
         for x in range(PAIR):
             for y in range(tp // 2):
-                both = terms[block, x, y, core].astype(F32) + near[block, x, y].astype(F32)
-                pair_sum[block, 0, x, y] = both[:, :lane_half].astype(BF16)
-                pair_sum[block, 1, x, y] = both[:, lane_half:].astype(BF16)
-        r_copy(1, block).start()
-        r_copy(2, block).start()
+                both = terms[u, x, y, core].astype(F32) + near[u, x, y].astype(F32)
+                pair_sum[u, 0, x, y] = both[:row_half].astype(BF16)
+                pair_sum[u, 1, x, y] = both[row_half:].astype(BF16)
+        r_copy(1, u).start()
+        r_copy(2, u).start()
 
     def pass_second(j):
-        block = block_at(j)
-        r_copy(1, block).wait_recv()
-        both = pair_sum[block, 0, side, 1 - row_y].astype(F32)
-        sum_x[block] = (both + first_x[block, 1 - row_y].astype(F32)).astype(BF16)
-        r_copy(3, block).start()
-        r_copy(2, block).wait_recv()
-        both = pair_sum[block, 1, 1 - side, row_y].astype(F32)
-        sum_y[block] = (both + first_y[block, 1 - side].astype(F32)).astype(BF16)
-        r_copy(4, block).start()
-
-    lag = 3
+        u = unit_of(j)
+        r_copy(1, u).wait_recv()
+        both = pair_sum[u, 0, side, 1 - row_y].astype(F32)
+        sum_x[u] = (both + first_x[u, 1 - row_y].astype(F32)).astype(BF16)
+        r_copy(3, u).start()
+        r_copy(2, u).wait_recv()
+        both = pair_sum[u, 1, 1 - side, row_y].astype(F32)
+        sum_y[u] = (both + first_y[u, 1 - side].astype(F32)).astype(BF16)
+        r_copy(4, u).start()
+
+    lag = 6
 
     def down(j, carry):
         pl.when(j >= lag)(lambda: pass_second(j - lag))
-        pl.when((j > 0) & (j < sp + 1))(lambda: pass_first(j - 1))
-        pl.when(j < sp)(lambda: produce(j))
+        pl.when((j > 0) & (j < units + 1))(lambda: pass_first(j - 1))
+        pl.when(j < units)(lambda: produce(j))
         return carry
 
-    lax.fori_loop(0, sp + lag, down, 0)
-
-    for block in range(sp):
-        r_copy(3, block).wait_recv()
-        r_copy(4, block).wait_recv()
+    lax.fori_loop(0, units + lag, down, 0)
+
+    for u in range(units):
+        r_copy(3, u).wait_recv()
+        r_copy(4, u).wait_recv()
+        lanes = pl.ds(u * unit, unit)
         for half in range(2):
-            first = first_x[block, row_y] if half == 0 else first_y[block, side]
-            last = last_x[block] if half == 0 else last_y[block]
-            lanes = pl.ds(block * cols + half * lane_half, lane_half)
-            acc = mid[:, lanes].astype(F32) + pair_sum[block, half, side, row_y].astype(F32)
+            rows = pl.ds(half * row_half, row_half)
+            first = first_x[u, row_y] if half == 0 else first_y[u, side]
+            last = last_x[u] if half == 0 else last_y[u]
+            acc = mid[rows, lanes].astype(F32) + pair_sum[u, half, side, row_y].astype(F32)
             acc = acc + first.astype(F32) + last.astype(F32)
-            out_ref[:, lanes] = acc.astype(BF16)
-
-    for kind in range(3):
+            out_ref[rows, lanes] = acc.astype(BF16)
+
+    for kind in range(2 + PAIR):
         w_copy(kind, me, 2, True).wait_send()
         for block in (me, mate):
             pl.when(can_down)(w_copy(kind, block, 0).wait_send)
@@ -801,7 +842,7 @@
 
     def drain(s, carry):
         there, above = step(s)
-        for kind in range(3):
+        for kind in range(2 + PAIR):
             for other in (False, True):
                 block = block_of(there, other)
                 pl.when(above & can_down)(w_copy(kind, block, 0).wait_send)
@@ -825,7 +866,7 @@
             r_copy(k, block).wait_send()
         return carry
 
-    lax.fori_loop(0, sp, drain_sums, 0)
+    lax.fori_loop(0, units, drain_sums, 0)
 
 
 def kernel_shards(
@@ -850,6 +891,8 @@
     heads = query.shape[1] // HD
     share = tok // tp
     wide = hid // PAIR
+    unit = cols // PAIR
+    units = PAIR * sp
     group = PAIR * tok
     inverse = THETA ** (-(np.arange(2 * HD) % (HD // 2)) * 2.0 / HD)
     local = (np.arange(tok + 2 * WINDOW) - WINDOW)[:, None] * inverse[None, :]
@@ -884,20 +927,20 @@
             pltpu.VMEM((group + 2 * EDGE, wide), F32),
             pltpu.VMEM((group + 2 * EDGE, wide), F32),
             pltpu.VMEM((group, wide), BF16),
-            pltpu.VMEM((sp, PAIR, tp // 2, 2, share, cols), BF16),
-            pltpu.VMEM((sp, PAIR, tp // 2, share, cols), BF16),
-            pltpu.VMEM((sp, 2, PAIR, tp // 2, share, cols // 2), BF16),
-            pltpu.VMEM((sp, tp // 2, share, cols // 2), BF16),
-            pltpu.VMEM((sp, PAIR, share, cols // 2), BF16),
-            pltpu.VMEM((sp, share, cols // 2), BF16),
-            pltpu.VMEM((sp, share, cols // 2), BF16),
-            pltpu.VMEM((sp, share, cols // 2), BF16),
-            pltpu.VMEM((sp, share, cols // 2), BF16),
+            pltpu.VMEM((units, PAIR, tp // 2, 2, share, unit), BF16),
+            pltpu.VMEM((units, PAIR, tp // 2, share, unit), BF16),
+            pltpu.VMEM((units, 2, PAIR, tp // 2, share // 2, unit), BF16),
+            pltpu.VMEM((units, tp // 2, share // 2, unit), BF16),
+            pltpu.VMEM((units, PAIR, share // 2, unit), BF16),
+            pltpu.VMEM((units, share // 2, unit), BF16),
+            pltpu.VMEM((units, share // 2, unit), BF16),
+            pltpu.VMEM((units, share // 2, unit), BF16),
+            pltpu.VMEM((units, share // 2, unit), BF16),
             pltpu.VMEM((3, wide), F32),
             pltpu.VMEM((3, wide), F32),
-            dma((7,)),
-            dma((3, sp, 3)),
-            dma((3, sp)),
+            dma((8,)),
+            dma((2 + PAIR, sp, 3)),
+            dma((2 + PAIR, sp)),
             dma((tp - 1,)),
             dma((tp,)),
             dma((tp - 1,)),
@@ -908,8 +951,8 @@
             dma((2, 2)),
             dma((9,)),
             dma((PAIR * tp, 2)),
-            dma((5, sp)),
-            dma((5, sp)),
+            dma((5, units)),
+            dma((5, units)),
         ],
         compiler_params=pltpu.CompilerParams(
             collective_id=0, has_side_effects=True, vmem_limit_bytes=62 * 1000 * 1000

time: 132 us -> 128 us (0.970)
  Pallas kernels: 131 us -> 127 us
    pallas_call x1, Pallas kernels: 131 us -> 127 us  [kernel_shards(): pl.pallas_call(functools.partial(layer_kernel, sp, tp), out_shape=pltpu.V...]
where the time goes in v3:
time: 128 us
  Pallas kernels  127 us (99%)
    pallas_call x1, Pallas kernels, kernel_shards(): pl.pallas_call(functools.partial(layer_kernel, sp, tp), out_shape=pltpu.V...  127 us

profile of v3, /device:TPU:0, one launch (start us, length us, event | category | flops | bytes accessed | tf_op | source)
XLA Modules:
  0.0 127.5 jit_solution(12157006824152414568)
XLA Ops:
  0.0 126.6 %layer.1 = bf16[256,2048]{1,0:T(8,128)(2,1)S(1)} custom-call(bf16[1024,256]{1,0:T(8,128)(2,1)} %q_ref.1, bf16[64,1024]{1,0:T(8,128)(2,1)} %bitcast.3, bf16[64,1024]{1,0:T(8,128)(2,1)} %bitcast.4, f32[2576,128]{1,0:T(8,128)} %constant.2.clone.table_ref, f32[4]{0:T(128)} %sink_ref.1, bf16[1024,2048]{1,0:T(8,128)(2,1)} %res_ref.1, f32[1,2048]{1,0:T(1,128)} %bitcast.5, ...), custom_call_target="tpu_custom_call" | custom-call | tf_op jit(solution)/shard_map/layer/pallas_call | solution.py:905
  126.6 1.0 copy.15

commit v4 on v3

--- a/solution.py
+++ b/solution.py
@@ -619,6 +619,12 @@
             for kind in range(2):
                 settle(s, kind, other)
 
+    n_wait(from_mate)
+    n_copy(4).start()
+    n_copy(3).start()
+    n_wait(from_across)
+    n_copy(6).start()
+    n_copy(5).start()
     for s in range(1, line - 1):
         settle_up(s)
     for kind in range(2):
@@ -626,12 +632,6 @@
     up_main(mine)
     n_wait(side * tp + buddy)
     up_main(side * tp + buddy)
-    n_wait(from_mate)
-    n_copy(4).start()
-    n_copy(3).start()
-    n_wait(from_across)
-    n_copy(6).start()
-    n_copy(5).start()
     up_main(from_mate)
     up_main(from_across)
     n_wait((1 - side) * tp + buddy)

time: 128 us -> 128 us (level)
  no operation moved by 1% of the time
where the time goes in v4:
time: 128 us
  Pallas kernels  127 us (99%)
    pallas_call x1, Pallas kernels, kernel_shards(): pl.pallas_call(functools.partial(layer_kernel, sp, tp), out_shape=pltpu.V...  127 us

profile of v4, /device:TPU:0, one launch (start us, length us, event | category | flops | bytes accessed | tf_op | source)
XLA Modules:
  0.0 127.5 jit_solution(7299041047663798952)
XLA Ops:
  0.0 126.6 %layer.1 = bf16[256,2048]{1,0:T(8,128)(2,1)S(1)} custom-call(bf16[1024,256]{1,0:T(8,128)(2,1)} %q_ref.1, bf16[64,1024]{1,0:T(8,128)(2,1)} %bitcast.3, bf16[64,1024]{1,0:T(8,128)(2,1)} %bitcast.4, f32[2576,128]{1,0:T(8,128)} %constant.2.clone.table_ref, f32[4]{0:T(128)} %sink_ref.1, bf16[1024,2048]{1,0:T(8,128)(2,1)} %res_ref.1, f32[1,2048]{1,0:T(1,128)} %bitcast.5, ...), custom_call_target="tpu_custom_call" | custom-call | tf_op jit(solution)/shard_map/layer/pallas_call | solution.py:905
  126.6 1.0 copy.15
